TPU v7x, 512 devices: a whole 4x8x8 slice. The times are simulated.
512 devices in a mesh: sp: 64 (over z, y), tp: 4 (over x), dp: 2 (over core).
Axes of the slice: x: 4, y: 8, z: 8, core: 2. Of those that a mesh axis runs over, the one named last changes fastest.
Arguments:
- latent: bfloat16 [2, 16384, 2048], P('dp', 'sp'), may hold values from -1.5 to 1.5
- condition: bfloat16 [2, 2048], P('dp', 'sp'), may hold values from -6 to 6
- context: bfloat16 [2, 1024, 2048], P('dp', 'sp'), may hold values from -6 to 6
- context_code: bfloat16 [2048], P('sp'), may hold values from -6 to 6
- shift_weight: bfloat16 [2048, 2048], P('sp', 'tp'), may hold values from -0.125 to 0.125
- scale_weight: bfloat16 [2048, 2048], P('sp', 'tp'), may hold values from -0.125 to 0.125
- gate_weight: bfloat16 [2048, 2048], P('sp', 'tp'), may hold values from -0.125 to 0.125
- norm_gain: float32 [2048], replicated, may hold values from 0.1 to 1.9
- query_weight: bfloat16 [2048, 1024], P(None, 'tp'), may hold values from -0.125 to 0.125
- key_weight: bfloat16 [2048, 256], P(None, 'tp'), may hold values from -0.125 to 0.125
- value_weight: bfloat16 [2048, 256], P(None, 'tp'), may hold values from -0.125 to 0.125
- output_weight: bfloat16 [1024, 2048], P('tp'), may hold values from -0.75 to 0.75
- query_gain: float32 [64], replicated, may hold values from 1 to 5.5
- key_gain: float32 [64], replicated, may hold values from 1 to 5.5
- context_bias: float32 [16], P('tp'), may hold values from 0.5 to 2
Outputs:
- updated: bfloat16 [2, 16384, 2048], P('dp', 'sp')
All inputs are finite; a program needn't handle non-finite values.
Results may differ from a plain program's by a relative error of at most 0.01405.
The roundings to bfloat16 on the way count: a program that leaves them out, or rounds other values in their place, can miss the bound.
Values may be sent and summed in bfloat16 or wider, within the bound.
A program may use at most 64 MiB of HBM per device.

v0:
```python
import math

import jax
import jax.numpy as jnp
from jax import lax
from jax.sharding import PartitionSpec as P

GRID_W = 64


norm_eps = 1e-06
rope_base = 10000.0


def from_everyone(array, axis):
    size = lax.axis_size(axis)
    return lax.all_to_all(
        jnp.broadcast_to(array[None], (size, *array.shape)), axis, 0, 0, tiled=True
    )


def of_everyone(array, axis):
    return from_everyone(array, axis).sum(axis=0)


def laid_out(pieces, dim):
    dims = list(pieces.shape[1:])
    dims[dim] *= pieces.shape[0]
    return jnp.moveaxis(pieces, 0, dim).reshape(dims)


def gathered_copies(array, axis, dim):
    pieces = from_everyone(array, axis)
    return laid_out(pieces, dim)


def cut_along(array, dim, size):
    before, after = (array.shape[:dim], array.shape[dim + 1 :])
    return jnp.moveaxis(array.reshape(*before, size, -1, *after), dim, 0)


def sent_and_summed(array, axis, dim):
    size = lax.axis_size(axis)
    pieces = lax.all_to_all(cut_along(array, dim, size), axis, 0, 0, tiled=True)
    return jnp.sum(pieces.astype(jnp.float32), axis=0)


def rotary_tables(position, grid_width, head_dim):
    grid_row = (position // grid_width).astype(jnp.float32)
    grid_col = (position % grid_width).astype(jnp.float32)
    quarter = head_dim // 4
    inverse = rope_base ** (-jnp.arange(quarter, dtype=jnp.float32) / quarter)
    angles = jnp.concatenate([grid_row[:, None] * inverse, grid_col[:, None] * inverse], axis=-1)
    return (jnp.cos(angles), jnp.sin(angles))


def head_norm(values, gain_row):
    return (
        values * lax.rsqrt(jnp.mean(values * values, axis=-1, keepdims=True) + norm_eps) * gain_row
    )


def rotate(values, cosine, sine_part):
    half_dim = values.shape[-1] // 2
    first_half = values[..., :half_dim]
    second_half = values[..., half_dim:]
    cos_rows = cosine[:, None, :]
    sin_rows = sine_part[:, None, :]
    return jnp.concatenate(
        [
            first_half * cos_rows - second_half * sin_rows,
            second_half * cos_rows + first_half * sin_rows,
        ],
        axis=-1,
    )


def modulated(tokens, gain_row, shift_row, scale_row):
    floats = tokens.astype(jnp.float32)
    normal = floats * lax.rsqrt(jnp.mean(floats * floats, axis=-1, keepdims=True) + norm_eps)
    return (normal * gain_row * (1.0 + scale_row) + shift_row).astype(jnp.bfloat16)


def on_device(
    latent,
    condition,
    context,
    context_code,
    shift_weight,
    scale_weight,
    gate_weight,
    norm_gain,
    query_weight,
    key_weight,
    value_weight,
    output_weight,
    query_gain,
    key_gain,
    context_bias,
):
    head_dim = query_gain.shape[0]
    tp_size = lax.axis_size("tp")
    activated = jax.nn.silu(condition[0].astype(jnp.float32)).astype(jnp.bfloat16)
    context_act = jax.nn.silu(context_code.astype(jnp.float32)).astype(jnp.bfloat16)
    partial_mod = jnp.stack(
        [
            jnp.dot(activated, shift_weight, preferred_element_type=jnp.float32),
            jnp.dot(activated, scale_weight, preferred_element_type=jnp.float32),
            jnp.dot(activated, gate_weight, preferred_element_type=jnp.float32),
            jnp.dot(context_act, shift_weight, preferred_element_type=jnp.float32),
            jnp.dot(context_act, scale_weight, preferred_element_type=jnp.float32),
        ]
    )
    summed = of_everyone(partial_mod, "sp")
    vectors = gathered_copies(summed, "tp", 1)
    normed = modulated(latent[0], norm_gain, vectors[0], vectors[1])
    query_cols = query_weight.shape[1]
    key_cols = key_weight.shape[1]
    projected = jnp.concatenate(
        [
            jnp.dot(normed, query_weight, preferred_element_type=jnp.float32),
            jnp.dot(normed, key_weight, preferred_element_type=jnp.float32),
            jnp.dot(normed, value_weight, preferred_element_type=jnp.float32),
        ],
        axis=1,
    )
    seq_rows = projected.shape[0]
    position = lax.axis_index("sp") * seq_rows + jnp.arange(seq_rows, dtype=jnp.int32)
    cosine, sine_part = rotary_tables(position, GRID_W, head_dim)
    group_size = query_cols // head_dim
    queries = projected[:, :query_cols].reshape(seq_rows, group_size, head_dim)
    queries = rotate(head_norm(queries, query_gain), cosine, sine_part).astype(jnp.bfloat16)
    latent_keys = projected[:, query_cols : query_cols + key_cols].reshape(seq_rows, 1, head_dim)
    latent_keys = rotate(head_norm(latent_keys, key_gain), cosine, sine_part).astype(jnp.bfloat16)
    latent_values = projected[:, query_cols + key_cols :].astype(jnp.bfloat16)
    key_value = jnp.concatenate([latent_keys.reshape(seq_rows, head_dim), latent_values], axis=1)
    context_normed = modulated(context[0], norm_gain, vectors[3], vectors[4])
    context_keys = head_norm(
        jnp.dot(context_normed, key_weight, preferred_element_type=jnp.float32), key_gain
    )
    context_values = jnp.dot(context_normed, value_weight, preferred_element_type=jnp.float32)
    context_kv = gathered_copies(
        jnp.concatenate(
            [context_keys.astype(jnp.bfloat16), context_values.astype(jnp.bfloat16)], axis=1
        ),
        "sp",
        0,
    )
    score_scale = head_dim ** (-0.5)
    query_rows = queries.transpose(1, 0, 2).reshape(group_size * seq_rows, head_dim)
    bias_rows = jnp.repeat(context_bias, seq_rows)
    context_scores = jnp.dot(
        query_rows, context_kv[:, :head_dim].T, preferred_element_type=jnp.float32
    )
    context_scores = context_scores * score_scale + bias_rows[:, None]
    first_max = context_scores.max(axis=1)
    context_exp = jnp.exp(context_scores - first_max[:, None])
    start_state = (
        first_max,
        context_exp.sum(axis=1),
        jnp.dot(
            context_exp.astype(jnp.bfloat16),
            context_kv[:, head_dim:],
            preferred_element_type=jnp.float32,
        ),
    )
    arrived = lax.all_gather(key_value, "sp", axis=0, tiled=True)
    arrived_rows = arrived.shape[0]
    block_rows = math.gcd(arrived_rows, 1024)
    blocks = arrived.reshape(arrived_rows // block_rows, block_rows, 2 * head_dim)

    def absorb_block(state_now, pair_block):
        old_max, old_total, old_accum = state_now
        scores = (
            jnp.dot(query_rows, pair_block[:, :head_dim].T, preferred_element_type=jnp.float32)
            * score_scale
        )
        new_max = jnp.maximum(old_max, scores.max(axis=1))
        factor = jnp.exp(old_max - new_max)
        weights = jnp.exp(scores - new_max[:, None])
        new_accum = old_accum * factor[:, None] + jnp.dot(
            weights.astype(jnp.bfloat16),
            pair_block[:, head_dim:],
            preferred_element_type=jnp.float32,
        )
        return ((new_max, old_total * factor + weights.sum(axis=1), new_accum), None)

    final_state, unused = lax.scan(absorb_block, start_state, blocks)
    row_max, totals, accum = final_state
    attended = (accum / totals[:, None]).astype(jnp.bfloat16)
    attended = (
        attended.reshape(group_size, seq_rows, head_dim)
        .transpose(1, 0, 2)
        .reshape(seq_rows, query_cols)
    )
    own_rows = seq_rows // tp_size
    mixed = sent_and_summed(
        jnp.dot(attended, output_weight, preferred_element_type=jnp.float32).astype(jnp.bfloat16),
        "tp",
        0,
    )
    own_latent = lax.dynamic_slice_in_dim(latent[0], lax.axis_index("tp") * own_rows, own_rows, 0)
    updated = (own_latent.astype(jnp.float32) + vectors[2] * mixed).astype(jnp.bfloat16)
    whole = gathered_copies(updated, "tp", 0)
    return whole[None]


def solution(mesh):
    return jax.shard_map(
        on_device,
        mesh=mesh,
        in_specs=(
            P("dp", "sp", None),
            P("dp", "sp"),
            P("dp", "sp", None),
            P("sp"),
            P("sp", "tp"),
            P("sp", "tp"),
            P("sp", "tp"),
            P(),
            P(None, "tp"),
            P(None, "tp"),
            P(None, "tp"),
            P("tp", None),
            P(),
            P(),
            P("tp"),
        ),
        out_specs=P("dp", "sp", None),
        check_vma=False,
    )
```

profile of v0, /device:TPU:8, one launch (start us, length us, event | category | flops | bytes accessed | tf_op | source)
XLA Modules:
  0.0 259.9 jit_solution(298645395595733858)
XLA Ops:
  6.5 1.0 fusion.59
  11.3 1.1 broadcast_in_dim.12
  12.4 16.6 %all-to-all-start = ((f32[64,5,512]{2,1,0:T(8,128)}), f32[64,5,512]{2,1,0:T(8,128)S(1)}, u32[]{:S(2)}, u32[]{:S(2)}) async-start(f32[64,5,512]{2,1,0:T(8,128)} %broadcast_in_dim.12), calls=%async_computation | async-start | bytes 2097152 | tf_op jit(solution)/shard_map/all_to_all | solution.py:17
  29.0 2.1 fusion.16
  31.2 27.1 %all-to-all-done = f32[64,5,512]{2,1,0:T(8,128)S(1)} async-done(((f32[64,5,512]{2,1,0:T(8,128)}), f32[64,5,512]{2,1,0:T(8,128)S(1)}, u32[]{:S(2)}, u32[]{:S(2)}) %all-to-all-start) | async-done | bytes 655392 | tf_op jit(solution)/shard_map/all_to_all | solution.py:17
  59.0 4.3 %all-to-all-start.1 = ((f32[4,5,512]{2,1,0:T(8,128)}), f32[4,5,512]{2,1,0:T(8,128)S(1)}, u32[]{:S(2)}, u32[]{:S(2)}) async-start(f32[4,5,512]{2,1,0:T(8,128)} %broadcast_in_dim.13), calls=%async_computation.1 | async-start | bytes 131072 | tf_op jit(solution)/shard_map/all_to_all | solution.py:17
  63.3 1.3 add_rsqrt_fusion.2
  64.6 4.3 %all-to-all-done.1 = f32[4,5,512]{2,1,0:T(8,128)S(1)} async-done(((f32[4,5,512]{2,1,0:T(8,128)}), f32[4,5,512]{2,1,0:T(8,128)S(1)}, u32[]{:S(2)}, u32[]{:S(2)}) %all-to-all-start.1) | async-done | bytes 40992 | tf_op jit(solution)/shard_map/all_to_all | solution.py:17
  69.5 1.6 convolution_convert_fusion.1
  71.2 1.3 multiply_reduce_fusion.2
  74.8 1.4 copy.33
  76.5 1.1 multiply_reduce_fusion.3
  78.3 1.2 convolution_convert_fusion.2
  80.3 7.0 %all-to-all-start.2 = ((bf16[64,16,128]{2,1,0:T(8,128)(2,1)}), bf16[64,16,128]{2,1,0:T(8,128)(2,1)S(1)}, u32[]{:S(2)}, u32[]{:S(2)}) async-start(bf16[64,16,128]{2,1,0:T(8,128)(2,1)} %broadcast_in_dim.14), calls=%async_computation.2 | async-start | bytes 524288 | tf_op jit(solution)/shard_map/all_to_all | solution.py:17
  87.3 2.0 multiply_reduce_fusion.1
  89.7 10.9 %all-to-all-done.2 = bf16[64,16,128]{2,1,0:T(8,128)(2,1)S(1)} async-done(((bf16[64,16,128]{2,1,0:T(8,128)(2,1)}), bf16[64,16,128]{2,1,0:T(8,128)(2,1)S(1)}, u32[]{:S(2)}, u32[]{:S(2)}) %all-to-all-start.2) | async-done | bytes 262176 | tf_op jit(solution)/shard_map/all_to_all | solution.py:17
  102.1 1.0 fusion.25
  103.1 57.5 %all-gather.2.cloned.1.call-done = bf16[16384,128]{0,1:T(8,128)(2,1)} async-done(((bf16[256,128]{0,1:T(8,128)(2,1)}), bf16[16384,128]{0,1:T(8,128)(2,1)}) %all-gather.2.cloned.1.call-update) | async-done | bytes 4194320 | tf_op jit(solution)/shard_map/all_gather | solution.py:167
  160.6 6.4 %copy.38 = bf16[16384,128]{1,0:T(8,128)(2,1)} copy(bf16[16384,128]{0,1:T(8,128)(2,1)} %all-gather.2.cloned.1.call-done) | data formatting | bytes 8388608 | tf_op jit(solution)/shard_map/while | solution.py:188
  167.0 54.7 %while.14 = (s32[]{:T(128)}, f32[1024]{0:T(1024)S(1)}, f32[1024]{0:T(1024)S(1)}, f32[1024,64]{0,1:T(8,128)S(1)}, bf16[16,1024,128]{2,1,0:T(8,128)(2,1)}, /*index=5*/bf16[1024,64]{1,0:T(8,128)(2,1)S(1)}, s32[]{:T(128)}) while((s32[]{:T(128)}, f32[1024]{0:T(1024)S(1)}, f32[1024]{0:T(1024)S(1)}, f32[1024,64]{0,1:T(8,128)S(1)}, ...), condition=%wide.region_11.12_spmd, body=%wide.region_8.11_spmd.sunk | while | flops 276957184 | bytes 14352473 | solution.py:188
  170.4 1.0 dynamic-slice_bitcast_fusion.2
  173.8 1.0 dynamic-slice_bitcast_fusion.2
  177.2 1.0 dynamic-slice_bitcast_fusion.2
  180.7 1.0 dynamic-slice_bitcast_fusion.2
  184.1 1.0 dynamic-slice_bitcast_fusion.2
  187.5 1.0 dynamic-slice_bitcast_fusion.2
  190.9 1.0 dynamic-slice_bitcast_fusion.2
  194.3 1.0 dynamic-slice_bitcast_fusion.2
  221.9 1.4 convolution_convert_fusion
  223.3 4.2 %all-to-all-start.3 = ((bf16[4,64,2048]{2,1,0:T(8,128)(2,1)}), bf16[4,64,2048]{2,1,0:T(8,128)(2,1)S(1)}, u32[]{:S(2)}, u32[]{:S(2)}) async-start(bf16[4,64,2048]{2,1,0:T(8,128)(2,1)} %bitcast.36), calls=%async_computation.3 | async-start | bytes 2097152 | tf_op jit(solution)/shard_map/all_to_all | solution.py:44
  227.5 10.9 %all-to-all-done.3 = bf16[4,64,2048]{2,1,0:T(8,128)(2,1)S(1)} async-done(((bf16[4,64,2048]{2,1,0:T(8,128)(2,1)}), bf16[4,64,2048]{2,1,0:T(8,128)(2,1)S(1)}, u32[]{:S(2)}, u32[]{:S(2)}) %all-to-all-start.3) | async-done | bytes 1048608 | tf_op jit(solution)/shard_map/all_to_all | solution.py:44
  238.8 13.3 %all_to_all.25 = bf16[4,64,2048]{2,1,0:T(8,128)(2,1)S(1)} all-to-all(bf16[4,64,2048]{2,1,0:T(8,128)(2,1)S(1)} %broadcast_in_dim.17), channel_id=1, replica_groups=mesh['sp'=64,'tp'=4,'dp'=2] {'tp'}, dimensions={0} | all-to-all | bytes 2097152 | tf_op jit(solution)/shard_map/all_to_all | solution.py:17
  (163 shorter events, 58.7 us)
Async XLA Ops:
  6.5 215.3 %copy-start = (bf16[256,2048]{1,0:T(8,128)(2,1)S(1)}, bf16[256,2048]{1,0:T(8,128)(2,1)}, u32[]{:S(2)}) copy-start(bf16[256,2048]{1,0:T(8,128)(2,1)} %param.28) | copy-start | bytes 3145732
  6.5 63.0 %copy-start.1 = (bf16[1,256,2048]{2,1,0:T(8,128)(2,1)S(1)}, bf16[1,256,2048]{2,1,0:T(8,128)(2,1)}, u32[]{:S(2)}) copy-start(bf16[1,256,2048]{2,1,0:T(8,128)(2,1)} %param.17) | copy-start | bytes 3145732
  11.2 59.9 %copy-start.4 = (bf16[2048,64]{0,1:T(8,128)(2,1)S(1)}, bf16[2048,64]{0,1:T(8,128)(2,1)}, u32[]{:S(2)}) copy-start(bf16[2048,64]{0,1:T(8,128)(2,1)} %param.26) | copy-start | bytes 786436
  12.4 45.9 %all-to-all-start = ((f32[64,5,512]{2,1,0:T(8,128)}), f32[64,5,512]{2,1,0:T(8,128)S(1)}, u32[]{:S(2)}, u32[]{:S(2)}) async-start(f32[64,5,512]{2,1,0:T(8,128)} %broadcast_in_dim.12), calls=%async_computation | async-start | bytes 2097152 | tf_op jit(solution)/shard_map/all_to_all | solution.py:17
  58.3 16.5 %copy-start.2 = (bf16[2048,256]{1,0:T(8,128)(2,1)S(1)}, bf16[2048,256]{1,0:T(8,128)(2,1)}, u32[]{:S(2)}) copy-start(bf16[2048,256]{1,0:T(8,128)(2,1)} %param.25) | copy-start | bytes 3145732
  59.0 9.9 %all-to-all-start.1 = ((f32[4,5,512]{2,1,0:T(8,128)}), f32[4,5,512]{2,1,0:T(8,128)S(1)}, u32[]{:S(2)}, u32[]{:S(2)}) async-start(f32[4,5,512]{2,1,0:T(8,128)} %broadcast_in_dim.13), calls=%async_computation.1 | async-start | bytes 131072 | tf_op jit(solution)/shard_map/all_to_all | solution.py:17
  63.3 97.3 %all-gather.2.cloned.1.call-start = ((), (), s32[]{:S(2)}) async-start(), calls=%async_computation.5 | async-start | bytes 4259840 | tf_op jit(solution)/shard_map/all_gather | solution.py:167
  69.5 3.9 %copy-start.6 = (f32[1,4,512]{2,0,1:T(1,128)}, f32[1,4,512]{2,0,1:T(1,128)S(1)}, u32[]{:S(2)}) copy-start(f32[1,4,512]{2,0,1:T(1,128)S(1)} %get-tuple-element.93) | copy-start | bytes 24580
  69.5 3.9 %copy-start.7 = (f32[1,4,512]{2,0,1:T(1,128)}, f32[1,4,512]{2,0,1:T(1,128)S(1)}, u32[]{:S(2)}) copy-start(f32[1,4,512]{2,0,1:T(1,128)S(1)} %get-tuple-element.94) | copy-start | bytes 24580
  69.5 6.8 %copy-start.3 = (bf16[1,16,2048]{2,1,0:T(8,128)(2,1)S(1)}, bf16[1,16,2048]{2,1,0:T(8,128)(2,1)}, u32[]{:S(2)}) copy-start(bf16[1,16,2048]{2,1,0:T(8,128)(2,1)} %param.19) | copy-start | bytes 196612
  74.8 14.5 %copy-start.8 = (f32[64]{0:T(128)S(1)}, f32[64]{0:T(128)}, u32[]{:S(2)}) copy-start(f32[64]{0:T(128)} %param.29) | copy-start | bytes 772
  80.3 20.2 %all-to-all-start.2 = ((bf16[64,16,128]{2,1,0:T(8,128)(2,1)}), bf16[64,16,128]{2,1,0:T(8,128)(2,1)S(1)}, u32[]{:S(2)}, u32[]{:S(2)}) async-start(bf16[64,16,128]{2,1,0:T(8,128)(2,1)} %broadcast_in_dim.14), calls=%async_computation.2 | async-start | bytes 524288 | tf_op jit(solution)/shard_map/all_to_all | solution.py:17
  221.7 16.9 %copy-start.5 = (f32[1,4,512]{2,0,1:T(1,128)S(1)}, f32[1,4,512]{2,0,1:T(1,128)}, u32[]{:S(2)}) copy-start(f32[1,4,512]{2,0,1:T(1,128)} %get-tuple-element.90) | copy-start | bytes 24580
  223.3 15.1 %all-to-all-start.3 = ((bf16[4,64,2048]{2,1,0:T(8,128)(2,1)}), bf16[4,64,2048]{2,1,0:T(8,128)(2,1)S(1)}, u32[]{:S(2)}, u32[]{:S(2)}) async-start(bf16[4,64,2048]{2,1,0:T(8,128)(2,1)} %bitcast.36), calls=%async_computation.3 | async-start | bytes 2097152 | tf_op jit(solution)/shard_map/all_to_all | solution.py:44
Sparse Core Ops, SparseCore 0:
  74.2 86.3 all-gather.1
where the time goes:
time: 261 us; the launch traced here: 260 us
  waiting for transfers between devices  111 us (43%)
  matrix products  41.4 us (16%)
  starting transfers between devices  32.1 us (12%)
  local copies, waits for them, and re-layouts  28 us (11%)
  other arithmetic  20 us (8%)
  between operations  13.7 us (5%)
  blocking collectives  13.3 us (5%)
    all_gather x1, waiting for transfers between devices, on_device(): arrived = lax.all_gather(key_value, 'sp', axis=0, tiled=True)  57.5 us
    all_to_all x3, waiting for transfers between devices, from_everyone(): lax.all_to_all(jnp.broadcast_to(array[None], (size, *array.shape)), axis,...  42.3 us
    all_to_all x3, starting transfers between devices, from_everyone(): lax.all_to_all(jnp.broadcast_to(array[None], (size, *array.shape)), axis,...  27.8 us
    squeeze x16, local copies, waits for them, and re-layouts, on_device(): final_state, unused = lax.scan(absorb_block, start_state, blocks)  15.5 us
    dot_general x16, matrix products, absorb_block(): jnp.dot(weights.astype(jnp.bfloat16), pair_block[:, head_dim:], preferred...  14.9 us
    all_to_all x1, blocking collectives, from_everyone(): lax.all_to_all(jnp.broadcast_to(array[None], (size, *array.shape)), axis,...  13.3 us
    reduce_sum x16, other arithmetic, absorb_block(): weights.sum(axis=1)  11.7 us
    dot_general x16, matrix products, absorb_block(): jnp.dot(query_rows, pair_block[:, :head_dim].T, preferred_element_type=jn...  11.5 us
  transfers between devices with their start and end apart: 5, of which 5 were waited for; matrix products, arithmetic and copies ran while one was open for 6% of the time, Pallas kernels for 0%

commit v1 on v0

v1 whole, which is shorter than its diff:
```python
import functools
import math

import jax
import jax.numpy as jnp
from jax import lax
from jax.experimental import pallas as pl
from jax.experimental.pallas import tpu as pltpu
from jax.sharding import PartitionSpec as P

MESH = pl.DeviceIdType.MESH
F32 = jnp.float32
BF16 = jnp.bfloat16
EPS = 1e-6
ROPE_BASE = 10000.0
GRID_W = 64
RING = 8
XN = 4
TOK = 256
CTXT = 16
D = 2048
HD = 64
NH = 4
QC = NH * HD
LOG2E = 1.4426950408889634


def dot(a, b):
    return jnp.dot(a, b, preferred_element_type=F32)


def kernel(
    latent_h, cond_h, context_h, code_h, shw_h, scw_h, gaw_h, ngain_h, wq_h, wk_h, wv_h, wo_h, qg_h, kg_h, bias_h,
    out_h,
    lat, cond, ctx, code, shw, scw, gaw, ngain, wq, wk, wv, wo, qg, kg, bias,
    outv, normed, wkv, qbd, qctx, bufa, bufb, mst, lst, acc, att,
    ma, ma_y, ma_s, ma_z, ma_x, mb, mb_z, mb_s, mb_y, mb_x,
    lsem, osem, sa, ra, sb, rb, smod, rmod, swo, rwo, satt, ratt,
):
    sp = lax.axis_index("sp")
    x = lax.axis_index("tp")
    d = lax.axis_index("dp")
    z = sp // RING
    y = sp % RING
    sgn = 1 - 2 * d

    def at_y(k):
        return {"sp": z * RING + lax.rem(y + k + 2 * RING, RING)}

    def at_z(k):
        return {"sp": lax.rem(z + k + 2 * RING, RING) * RING + y}

    def at_x(k):
        return {"tp": lax.rem(x + k + 2 * XN, XN)}

    partner = {"dp": 1 - d}

    def remote(src, dst, ss, rs, dev):
        return pltpu.make_async_remote_copy(
            src_ref=src, dst_ref=dst, send_sem=ss, recv_sem=rs, device_id=dev, device_id_type=MESH
        )

    pairs = [
        (cond_h, cond), (code_h, code), (shw_h, shw), (scw_h, scw), (gaw_h, gaw),
        (latent_h, lat), (context_h, ctx), (ngain_h, ngain), (wk_h, wk), (wv_h, wv), (wq_h, wq),
        (qg_h, qg), (kg_h, kg), (bias_h, bias),
        (wo_h.at[:, 0 : D // 2], wo.at[x, 0]), (wo_h.at[:, D // 2 : D], wo.at[x, 1]),
    ]
    loads = [pltpu.make_async_copy(s, t, lsem.at[i]) for i, (s, t) in enumerate(pairs)]
    for c in loads:
        c.start()

    barrier = pltpu.get_barrier_semaphore()
    for k in range(1, RING):
        pl.semaphore_signal(barrier, inc=1, device_id=at_y(k), device_id_type=MESH)
        pl.semaphore_signal(barrier, inc=1, device_id=at_z(k), device_id_type=MESH)
    for k in range(1, XN):
        pl.semaphore_signal(barrier, inc=1, device_id=at_x(k), device_id_type=MESH)
    pl.semaphore_signal(barrier, inc=1, device_id=partner, device_id_type=MESH)

    for i in range(5):
        loads[i].wait()
    both = jnp.concatenate([cond[...], code[...]], axis=0).astype(F32)
    act = (both * (1.0 / (1.0 + jnp.exp(-both)))).astype(BF16)
    pshift = dot(act, shw[...])
    pscale = dot(act, scw[...])
    pgate = dot(act, gaw[...])
    for c in range(4):
        cols = slice(c * 128, (c + 1) * 128)
        ma[c : c + 1, :] = pshift[0:1, cols]
        ma[4 + c : 5 + c, :] = pscale[0:1, cols]
        ma[8 + c : 9 + c, :] = pgate[0:1, cols]
        mb[c : c + 1, :] = pshift[1:2, cols]
        mb[4 + c : 5 + c, :] = pscale[1:2, cols]
    ma[12:16, :] = jnp.zeros((4, 128), F32)

    pl.semaphore_wait(barrier, 2 * (RING - 1) + (XN - 1) + 1)

    def xa(src, dst, base, dev, k):
        return remote(src, dst.at[k], smod.at[base + k], rmod.at[base + k], dev)

    p1 = []
    for k in range(1, RING):
        p1.append(xa(ma, ma_y, 0, at_y(k), k))
        p1.append(xa(mb, mb_z, 8, at_z(k), k))
    for c in p1:
        c.start()

    for i in (14, 15):
        loads[i].wait()
    wo1 = [
        remote(wo.at[x, d], wo.at[x, d], swo.at[0], rwo.at[0], at_x(1)),
        remote(wo.at[x, d], wo.at[x, d], swo.at[1], rwo.at[1], at_x(-1)),
    ]
    for c in wo1:
        c.start()

    for i in (5, 6, 7, 8, 9):
        loads[i].wait()
    lf = lat[...].astype(F32)
    rms = lax.rsqrt(jnp.mean(lf * lf, axis=-1, keepdims=True) + EPS)
    cf = ctx[...].astype(F32)
    crms = lax.rsqrt(jnp.mean(cf * cf, axis=-1, keepdims=True) + EPS)
    wkv[...] = jnp.concatenate([wk[...], wv[...]], axis=1)
    qbd[...] = jnp.zeros(qbd.shape, BF16)
    qctx[...] = jnp.zeros(qctx.shape, BF16)
    mst[...] = jnp.full(mst.shape, -1e30, F32)
    lst[...] = jnp.zeros(lst.shape, F32)
    acc[...] = jnp.zeros(acc.shape, F32)
    fi = lax.broadcasted_iota(jnp.int32, (32, TOK), 0)
    ti = lax.broadcasted_iota(jnp.int32, (32, TOK), 1)
    grow = sp * (TOK // GRID_W) + ti // GRID_W
    gcol = ti % GRID_W
    gpos = jnp.where(fi < 16, grow, gcol).astype(F32)
    inv = jnp.exp((fi % 16).astype(F32) * (-math.log(ROPE_BASE) / 16.0))
    angle = gpos * inv
    cosv = jnp.cos(angle)
    sinv = jnp.sin(angle)

    for c in p1:
        c.wait()
    ta = ma[...]
    tb = mb[...]
    for k in range(1, RING):
        ta = ta + ma_y[k]
        tb = tb + mb_z[k]
    ma_s[0] = ta
    mb_s[0] = tb
    p2 = []
    for k in range(1, RING):
        p2.append(xa(ma_s.at[0], ma_z, 16, at_z(k), k))
        p2.append(xa(mb_s.at[0], mb_y, 24, at_y(k), k))
    for c in p2:
        c.start()
    for c in p2:
        c.wait()
    for k in range(1, RING):
        ta = ta + ma_z[k]
        tb = tb + mb_y[k]
    ma_x[x] = ta
    mb_x[x] = tb
    p3 = []
    for k in range(1, XN):
        p3.append(remote(ma_x.at[x], ma_x.at[x], smod.at[32 + k], rmod.at[32 + k], at_x(k)))
        p3.append(remote(mb_x.at[x], mb_x.at[x], smod.at[36 + k], rmod.at[36 + k], at_x(k)))
    for c in p3:
        c.start()
    for c in p3:
        c.wait()

    def vec(ref, row):
        return jnp.concatenate([ref[i, row + c : row + c + 1, :] for i in range(XN) for c in range(4)], axis=1)

    gain = ngain[...]
    lshift = vec(ma_x, 0)
    lscale = gain * (1.0 + vec(ma_x, 4))
    cshift = vec(mb_x, 0)
    cscale = gain * (1.0 + vec(mb_x, 4))
    normed[0:TOK, :] = (lat[...].astype(F32) * rms * lscale + lshift).astype(BF16)
    normed[TOK : TOK + CTXT, :] = (cf * crms * cscale + cshift).astype(BF16)

    kv = dot(normed[...], wkv[...])
    kvt = kv[0:TOK, :].T
    for i in (10, 11, 12, 13):
        loads[i].wait()
    eye = lax.broadcasted_iota(jnp.int32, (HD, HD), 0) == lax.broadcasted_iota(jnp.int32, (HD, HD), 1)
    qgain = jnp.sum(jnp.where(eye, qg[...], 0.0), axis=1, keepdims=True)
    kgain = jnp.sum(jnp.where(eye, kg[...], 0.0), axis=1, keepdims=True)

    def norm_rope(t, g):
        t = t * lax.rsqrt(jnp.mean(t * t, axis=0, keepdims=True) + EPS) * g
        a, b = t[0:32, :], t[32:64, :]
        return jnp.concatenate([a * cosv - b * sinv, b * cosv + a * sinv], axis=0)

    kt = norm_rope(kvt[0:HD, :], kgain)
    k2 = jnp.concatenate([kt, kt], axis=0).T
    low = lax.broadcasted_iota(jnp.int32, (HD, 128), 1) < HD
    vt = kvt[HD : 2 * HD, :].astype(BF16)
    bufa[0, 0:64, :] = jnp.where(low, k2[0:64], k2[64:128]).astype(BF16)
    bufb[0, 0:64, :] = jnp.where(low, k2[128:192], k2[192:256]).astype(BF16)
    bufa[0, 64:128, :] = vt[:, 0:128]
    bufb[0, 64:128, :] = vt[:, 128:256]
    ckv = kv[TOK : TOK + CTXT, :]
    lowc = lax.broadcasted_iota(jnp.int32, (CTXT, 128), 1) < HD
    csq = jnp.sum(jnp.where(lowc, ckv * ckv, 0.0), axis=1, keepdims=True) * (1.0 / HD)
    kg2 = jnp.concatenate([kg[...], kg[...]], axis=1)
    bufa[0, 128:144, :] = jnp.where(lowc, ckv * lax.rsqrt(csq + EPS) * kg2, ckv).astype(BF16)

    def send(src, dst, dev_a, dev_b):
        remote(bufa.at[src], bufa.at[dst], sa.at[dst], ra.at[dst], dev_a).start()
        remote(bufb.at[src], bufb.at[dst], sb.at[dst], rb.at[dst], dev_b).start()

    def arrived(s):
        remote(bufa.at[s], bufa.at[s], sa.at[s], ra.at[s], at_z(1)).wait_recv()
        remote(bufb.at[s], bufb.at[s], sb.at[s], rb.at[s], at_y(1)).wait_recv()

    def first(dst_, src_, s):
        send(src_, dst_, at_y(s), at_z(s))

    def second(src_, dst_, s):
        send(src_, dst_, at_z(s), at_y(s))

    def start_rows(i):
        nxt = {0: (1, 2), 1: (3,), 2: (4,), 3: (5,), 4: (6,), 5: (7,)}.get(i, ())
        for t in nxt:
            first(t, i, sgn if t % 2 == 1 else -sgn)
        base = (2 + i // 2) * 4 + i % 2
        second(i, base, sgn)
        second(i, base + 2, -sgn)

    start_rows(0)

    q = dot(normed[0:TOK, :], wq[...])
    qt = q.T
    for h in range(NH):
        qh = norm_rope(qt[h * HD : (h + 1) * HD, :], qgain).astype(BF16)
        qs = qh.astype(F32) * (LOG2E * HD**-0.5)
        hi = qs.astype(BF16)
        lo = (qs - hi.astype(F32)).astype(BF16)
        for t in range(2):
            cols = slice(t * 128, (t + 1) * 128)
            for r, part in ((0, hi), (128, lo)):
                qbd[2 * h + t, r : r + 64, 0:128] = part[:, cols]
                qbd[2 * h + t, r + 64 : r + 128, 128:256] = part[:, cols]
        qctx[h, 0:64, :] = hi
        qctx[h, 128:192, :] = lo

    def absorb(h, mnew, rowsum, prod):
        alpha = jnp.exp2(mst[h] - mnew)
        mst[h] = mnew
        lst[h] = lst[h] * alpha[0:1, :] + rowsum
        acc[h] = acc[h] * alpha[0:1, :] + prod

    def step(it, carry):
        base = it * 4

        @pl.when(it == 0)
        def _():
            for i in (1, 2, 3):
                arrived(i)
                start_rows(i)

        @pl.when(it == 1)
        def _():
            for i in (4, 5, 6, 7):
                arrived(i)
                start_rows(i)

        @pl.when((it >= 2) & (it < 10))
        def _():
            for k in range(4):
                arrived(base + k)
                second(base + k, base + k + 16, sgn if k < 2 else -sgn)

        @pl.when((it >= 10) & (it < 14))
        def _():
            for k in range(4):
                arrived(base + k)
                if k < 2:
                    second(base + k, 56 + 2 * (it - 10) + k, sgn)

        @pl.when(it >= 14)
        def _():
            for k in range(4):
                arrived(base + k)

        @pl.when(it == 8)
        def _():
            for c in wo1:
                c.wait()
            left = lax.rem(x + XN - 1, XN)
            right = lax.rem(x + 1, XN)
            remote(wo.at[left, d, 0:128], wo.at[left, d, 0:128], swo.at[2], rwo.at[2], at_x(1)).start()
            remote(wo.at[right, d, 128:256], wo.at[right, d, 128:256], swo.at[3], rwo.at[3], at_x(-1)).start()
            remote(wo.at[left, d], wo.at[left, d], swo.at[4], rwo.at[4], partner).start()
            remote(wo.at[right, d], wo.at[right, d], swo.at[5], rwo.at[5], partner).start()

        @pl.when(it == 14)
        def _():
            far = lax.rem(x + 2, XN)
            remote(wo.at[far, d, 0:128], wo.at[far, d, 0:128], swo.at[2], rwo.at[2], at_x(1)).wait()
            remote(wo.at[far, d, 128:256], wo.at[far, d, 128:256], swo.at[3], rwo.at[3], at_x(-1)).wait()
            remote(wo.at[far, d], wo.at[far, d], swo.at[6], rwo.at[6], partner).start()

        keys = jnp.concatenate(
            [bufa[pl.ds(base, 4), 0:64, :].reshape(256, 128), bufb[pl.ds(base, 4), 0:64, :].reshape(256, 128)], axis=0
        )
        keys = jnp.concatenate([keys, keys], axis=1)
        vals = jnp.concatenate(
            [bufa[base + k, 64:128, :] for k in range(4)] + [bufb[base + k, 64:128, :] for k in range(4)], axis=1
        )
        for h in range(NH):
            ps = []
            ms = []
            sums = []
            mold = mst[h]
            for t in range(2):
                s = dot(keys, qbd[2 * h + t])
                m = jnp.max(s.reshape(64, 8, 256), axis=0)
                m = jnp.maximum(m[:, 0:128], m[:, 128:256])
                m = jnp.max(m, axis=0, keepdims=True)
                m = jnp.maximum(m, mold[0:1, t * 128 : (t + 1) * 128])
                e = jnp.exp2(s - jnp.concatenate([m, m], axis=1))
                r = jnp.sum(e.reshape(64, 8, 256), axis=0)
                sums.append(r[:, 0:128] + r[:, 128:256])
                ms.append(m)
                pb = e.astype(BF16)
                parts = []
                for k in range(8):
                    parts.append(pb[64 * k : 64 * k + 64, 0:128])
                    parts.append(pb[64 * k : 64 * k + 64, 128:256])
                ps.append(jnp.concatenate(parts, axis=0))
            prod = dot(vals, jnp.concatenate(ps, axis=1))
            mnew = jnp.broadcast_to(jnp.concatenate(ms, axis=1), (8, 256))
            absorb(h, mnew, jnp.concatenate(sums, axis=1), prod)

        @pl.when(it % 4 == 3)
        def _():
            c = bufa[pl.ds(base - 12, 16), 128:144, :].reshape(256, 128)
            cc = jnp.concatenate([c, c], axis=1)
            cvt = c.astype(F32).T[HD:128, :].astype(BF16)
            for h in range(NH):
                s = dot(cc, qctx[h]) + bias[0:1, h : h + 1] * LOG2E
                mold = mst[h]
                m = jnp.maximum(jnp.max(s, axis=0, keepdims=True), mold[0:1, :])
                e = jnp.exp2(s - m)
                r = jnp.sum(e.reshape(32, 8, 256), axis=0)
                prod = dot(cvt, e.astype(BF16))
                absorb(h, jnp.broadcast_to(m, (8, 256)), r, prod)

        return carry

    lax.fori_loop(0, 16, step, 0)

    heads = []
    for h in range(NH):
        total = jnp.sum(lst[h], axis=0, keepdims=True)
        heads.append(acc[h] / total)
    att[x] = jnp.concatenate(heads, axis=0).T.astype(BF16)

    left = lax.rem(x + XN - 1, XN)
    right = lax.rem(x + 1, XN)
    far = lax.rem(x + 2, XN)

    def att_copy(slot, half, sem, k):
        part = att.at[slot, half * 128 : half * 128 + 128]
        return remote(part, part, satt.at[sem], ratt.at[sem], at_x(k))

    own = [att_copy(x, 0, 0, 1), att_copy(x, 1, 1, -1), att_copy(x, 1, 2, 1), att_copy(x, 0, 3, -1)]
    for c in own:
        c.start()
    own[0].wait_recv()
    fwd0 = att_copy(left, 0, 4, 1)
    fwd0.start()
    own[1].wait_recv()
    fwd1 = att_copy(right, 1, 5, -1)
    fwd1.start()
    own[2].wait_recv()
    own[3].wait_recv()
    for s, slot in ((4, left), (5, right), (6, far)):
        remote(wo.at[slot, d], wo.at[slot, d], swo.at[s], rwo.at[s], partner).wait()
    fwd0.wait()
    fwd1.wait()

    gate = vec(ma_x, 8)
    outs = []
    for c in range(8):
        side, off = c // 4, (c % 4) * 256
        mixed = jnp.zeros((TOK, 256), F32)
        for g in range(XN):
            mixed = mixed + dot(att[g], wo[g, side, :, off : off + 256]).astype(BF16).astype(F32)
        cols = slice(c * 256, (c + 1) * 256)
        outv[:, cols] = (lat[:, cols].astype(F32) + gate[:, cols] * mixed).astype(BF16)
        o = pltpu.make_async_copy(outv.at[:, cols], out_h.at[:, cols], osem.at[c])
        o.start()
        outs.append(o)

    for c in own:
        c.wait_send()

    def drain(s, carry):
        remote(bufa.at[s], bufa.at[s], sa.at[s], ra.at[s], at_z(1)).wait_send()
        remote(bufb.at[s], bufb.at[s], sb.at[s], rb.at[s], at_y(1)).wait_send()
        return carry

    lax.fori_loop(1, 64, drain, 0)
    for o in outs:
        o.wait()


def on_device(
    latent, condition, context, context_code, shift_weight, scale_weight, gate_weight, norm_gain,
    query_weight, key_weight, value_weight, output_weight, query_gain, key_gain, context_bias,
):
    V = pltpu.VMEM
    dma = pltpu.SemaphoreType.DMA
    scratch = [
        V((TOK, D), BF16), V((1, 32), BF16), V((CTXT, D), BF16), V((1, 32), BF16),
        V((32, 512), BF16), V((32, 512), BF16), V((32, 512), BF16), V((1, D), F32),
        V((D, QC), BF16), V((D, HD), BF16), V((D, HD), BF16), V((XN, 2, QC, D // 2), BF16),
        V((1, HD), F32), V((1, HD), F32), V((1, NH), F32),
        V((TOK, D), BF16), V((TOK + CTXT, D), BF16), V((D, 128), BF16),
        V((8, 256, 256), BF16), V((NH, 256, 256), BF16),
        V((64, 144, 128), BF16), V((64, 128, 128), BF16),
        V((NH, 8, 256), F32), V((NH, 8, 256), F32), V((NH, HD, 256), F32), V((XN, TOK, QC), BF16),
        V((16, 128), F32), V((RING, 16, 128), F32), V((1, 16, 128), F32), V((RING, 16, 128), F32), V((XN, 16, 128), F32),
        V((8, 128), F32), V((RING, 8, 128), F32), V((1, 8, 128), F32), V((RING, 8, 128), F32), V((XN, 8, 128), F32),
        dma((16,)), dma((8,)), dma((64,)), dma((64,)), dma((64,)), dma((64,)),
        dma((40,)), dma((40,)), dma((8,)), dma((8,)), dma((8,)), dma((8,)),
    ]
    out = pl.pallas_call(
        kernel,
        out_shape=jax.ShapeDtypeStruct((TOK, D), BF16),
        in_specs=[pl.BlockSpec(memory_space=pl.ANY)] * 15,
        out_specs=pl.BlockSpec(memory_space=pl.ANY),
        scratch_shapes=scratch,
        compiler_params=pltpu.CompilerParams(
            collective_id=0, has_side_effects=True, vmem_limit_bytes=60 * 1024 * 1024
        ),
        name="fused",
    )(
        latent[0], condition, context[0], context_code[None], shift_weight, scale_weight, gate_weight,
        norm_gain[None], query_weight, key_weight, value_weight, output_weight,
        query_gain[None], key_gain[None], context_bias[None],
    )
    return out[None]


def solution(mesh):
    return jax.shard_map(
        on_device,
        mesh=mesh,
        in_specs=(
            P("dp", "sp", None), P("dp", "sp"), P("dp", "sp", None), P("sp"),
            P("sp", "tp"), P("sp", "tp"), P("sp", "tp"), P(),
            P(None, "tp"), P(None, "tp"), P(None, "tp"), P("tp", None),
            P(), P(), P("tp"),
        ),
        out_specs=P("dp", "sp", None),
        check_vma=False,
    )
```

time: 261 us -> 101 us (0.39)
  the two profiles are of different devices: /device:TPU:8 before, /device:TPU:4 now
where the time goes in v1:
time: 101 us
  Pallas kernels  95.4 us (94%)
  local copies, waits for them, and re-layouts  5.33 us (5%)
    pallas_call x1, Pallas kernels, on_device(): pl.pallas_call(kernel, out_shape=jax.ShapeDtypeStruct((TOK, D), BF16), in...  95.4 us
    unnamed x5, local copies, waits for them, and re-layouts  5.33 us

profile of v1, /device:TPU:4, one launch (start us, length us, event | category | flops | bytes accessed | tf_op | source)
XLA Modules:
  0.0 100.8 jit_solution(2086520260747265469)
XLA Ops:
  0.0 0.0 copy-start
  0.0 2.0 %copy.16.wk_h = bf16[2048,64]{1,0:T(8,128)(2,1)} copy(bf16[2048,64]{0,1:T(8,128)(2,1)} %param.24) | data formatting | bytes 524288 | tf_op args[9]
  2.0 0.0 copy-done
  2.0 1.0 %copy.17.wv_h = bf16[2048,64]{1,0:T(8,128)(2,1)} copy(bf16[2048,64]{0,1:T(8,128)(2,1)S(1)} %copy-done) | data formatting | bytes 524288 | tf_op args[10]
  3.0 95.4 %fused.1 = bf16[256,2048]{1,0:T(8,128)(2,1)} custom-call(bf16[256,2048]{1,0:T(8,128)(2,1)} %bitcast.9, bf16[1,32]{1,0:T(2,128)(2,1)} %cond_h.1, bf16[16,2048]{1,0:T(8,128)(2,1)} %bitcast.10, bf16[1,32]{1,0:T(2,128)(2,1)} %bitcast.12, bf16[32,512]{1,0:T(8,128)(2,1)} %shw_h.1, bf16[32,512]{1,0:T(8,128)(2,1)} %scw_h.1, bf16[32,512]{1,0:T(8,128)(2,1)} %gaw_h.1, ...), custom_call_target="tpu_custom_call" | custom-call | tf_op jit(solution)/shard_map/fused/pallas_call | solution.py:431
  98.5 2.3 %copy.19 = bf16[1,256,2048]{2,1,0:T(8,128)(2,1)} copy(bf16[1,256,2048]{2,1,0:T(8,128)(2,1)} %bitcast.8) | data formatting | bytes 2097152
Async XLA Ops:
  0.0 2.0 %copy-start = (bf16[2048,64]{0,1:T(8,128)(2,1)S(1)}, bf16[2048,64]{0,1:T(8,128)(2,1)}, u32[]{:S(2)}) copy-start(bf16[2048,64]{0,1:T(8,128)(2,1)} %param.25) | copy-start | bytes 786436

commit v2 on v1

--- a/solution.py
+++ b/solution.py
@@ -25,6 +25,29 @@
 LOG2E = 1.4426950408889634
 
 
+ORDER = [
+    (0, 0), (1, 0), (2, 0), (0, -1), (0, 1), (4, 0), (3, 0), (1, 1), (1, -1), (2, -1), (2, 1), (0, 2), (0, -2),
+    (5, 0), (6, 0), (3, -1), (3, 1), (4, -1), (4, 1), (1, 2), (1, -2), (5, -1), (7, 0), (5, 1), (6, -1), (2, -2),
+    (6, 1), (3, -2), (2, 2), (7, -1), (7, 1), (4, -2), (3, 2), (5, -2), (4, 2), (6, -2), (5, 2), (7, -2), (6, 2),
+    (0, -3), (7, 2), (1, -3), (0, 3), (1, 3), (2, -3), (3, -3), (2, 3), (4, -3), (3, 3), (4, 3), (5, -3), (5, 3),
+    (6, -3), (7, -3), (6, 3), (7, 3), (0, 4), (1, 4), (2, 4), (3, 4), (4, 4), (5, 4), (6, 4), (7, 4),
+]
+SLOT = {item: n for n, item in enumerate(ORDER)}
+NEXT = {0: ((1, 1), (2, -1)), 1: ((3, 1),), 2: ((4, -1),), 3: ((5, 1),), 4: ((6, -1),), 5: ((7, 1),)}
+
+
+def onward(item):
+    i, r = item
+    out = []
+    if r == 0:
+        out += [(0, way, SLOT[(j, 0)]) for j, way in NEXT.get(i, ())]
+    if 0 <= r < 4:
+        out.append((1, 1, SLOT[(i, r + 1)]))
+    if -3 < r <= 0:
+        out.append((1, -1, SLOT[(i, r - 1)]))
+    return out
+
+
 def dot(a, b):
     return jnp.dot(a, b, preferred_element_type=F32)
 
@@ -32,8 +55,8 @@
 def kernel(
     latent_h, cond_h, context_h, code_h, shw_h, scw_h, gaw_h, ngain_h, wq_h, wk_h, wv_h, wo_h, qg_h, kg_h, bias_h,
     out_h,
-    lat, cond, ctx, code, shw, scw, gaw, ngain, wq, wk, wv, wo, qg, kg, bias,
-    outv, normed, wkv, qbd, qctx, bufa, bufb, mst, lst, acc, att,
+    lat, cond, ctx, code, shw, scw, gaw, ngain, wq, wkv, wo, qg, kg, bias,
+    outv, normed, qbd, qctx, bufa, bufb, mst, alp, lst, acc, att, sbuf0, sbuf1, sctx,
     ma, ma_y, ma_s, ma_z, ma_x, mb, mb_z, mb_s, mb_y, mb_x,
     lsem, osem, sa, ra, sb, rb, smod, rmod, swo, rwo, satt, ratt,
 ):
@@ -62,7 +85,7 @@
 
     pairs = [
         (cond_h, cond), (code_h, code), (shw_h, shw), (scw_h, scw), (gaw_h, gaw),
-        (latent_h, lat), (context_h, ctx), (ngain_h, ngain), (wk_h, wk), (wv_h, wv), (wq_h, wq),
+        (latent_h, lat), (context_h, ctx), (ngain_h, ngain), (wk_h, wkv.at[0:HD]), (wv_h, wkv.at[HD : 2 * HD]), (wq_h, wq),
         (qg_h, qg), (kg_h, kg), (bias_h, bias),
         (wo_h.at[:, 0 : D // 2], wo.at[x, 0]), (wo_h.at[:, D // 2 : D], wo.at[x, 1]),
     ]
@@ -96,15 +119,16 @@
 
     pl.semaphore_wait(barrier, 2 * (RING - 1) + (XN - 1) + 1)
 
-    def xa(src, dst, base, dev, k):
-        return remote(src, dst.at[k], smod.at[base + k], rmod.at[base + k], dev)
-
-    p1 = []
-    for k in range(1, RING):
-        p1.append(xa(ma, ma_y, 0, at_y(k), k))
-        p1.append(xa(mb, mb_z, 8, at_z(k), k))
-    for c in p1:
-        c.start()
+    def spread(src, dst, sem, at):
+        for k in range(1, RING):
+            remote(src, dst.at[k], smod.at[sem], rmod.at[sem], at(k)).start()
+
+    def spread_wait(dst, sem):
+        part = dst.at[1:RING]
+        remote(part, part, smod.at[sem], rmod.at[sem], at_y(1)).wait()
+
+    spread(ma, ma_y, 0, at_y)
+    spread(mb, mb_z, 1, at_z)
 
     for i in (14, 15):
         loads[i].wait()
@@ -121,7 +145,6 @@
     rms = lax.rsqrt(jnp.mean(lf * lf, axis=-1, keepdims=True) + EPS)
     cf = ctx[...].astype(F32)
     crms = lax.rsqrt(jnp.mean(cf * cf, axis=-1, keepdims=True) + EPS)
-    wkv[...] = jnp.concatenate([wk[...], wv[...]], axis=1)
     qbd[...] = jnp.zeros(qbd.shape, BF16)
     qctx[...] = jnp.zeros(qctx.shape, BF16)
     mst[...] = jnp.full(mst.shape, -1e30, F32)
@@ -137,8 +160,8 @@
     cosv = jnp.cos(angle)
     sinv = jnp.sin(angle)
 
-    for c in p1:
-        c.wait()
+    spread_wait(ma_y, 0)
+    spread_wait(mb_z, 1)
     ta = ma[...]
     tb = mb[...]
     for k in range(1, RING):
@@ -146,28 +169,21 @@
         tb = tb + mb_z[k]
     ma_s[0] = ta
     mb_s[0] = tb
-    p2 = []
-    for k in range(1, RING):
-        p2.append(xa(ma_s.at[0], ma_z, 16, at_z(k), k))
-        p2.append(xa(mb_s.at[0], mb_y, 24, at_y(k), k))
-    for c in p2:
-        c.start()
-    for c in p2:
-        c.wait()
+    spread(ma_s.at[0], ma_z, 2, at_z)
+    spread(mb_s.at[0], mb_y, 3, at_y)
+    spread_wait(ma_z, 2)
+    spread_wait(mb_y, 3)
     for k in range(1, RING):
         ta = ta + ma_z[k]
         tb = tb + mb_y[k]
     ma_x[x] = ta
     mb_x[x] = tb
-    p3 = []
     for k in range(1, XN):
-        p3.append(remote(ma_x.at[x], ma_x.at[x], smod.at[32 + k], rmod.at[32 + k], at_x(k)))
-        p3.append(remote(mb_x.at[x], mb_x.at[x], smod.at[36 + k], rmod.at[36 + k], at_x(k)))
-    for c in p3:
-        c.start()
-    for c in p3:
-        c.wait()
-
+        remote(ma_x.at[x], ma_x.at[x], smod.at[4], rmod.at[4], at_x(k)).start()
+        remote(mb_x.at[x], mb_x.at[x], smod.at[5], rmod.at[5], at_x(k)).start()
+    for ref, sem in ((ma_x, 4), (mb_x, 5)):
+        part = ref.at[1:XN]
+        remote(part, part, smod.at[sem], rmod.at[sem], at_x(1)).wait()
     def vec(ref, row):
         return jnp.concatenate([ref[i, row + c : row + c + 1, :] for i in range(XN) for c in range(4)], axis=1)
 
@@ -179,7 +195,7 @@
     normed[0:TOK, :] = (lat[...].astype(F32) * rms * lscale + lshift).astype(BF16)
     normed[TOK : TOK + CTXT, :] = (cf * crms * cscale + cshift).astype(BF16)
 
-    kv = dot(normed[...], wkv[...])
+    kv = lax.dot_general(normed[...], wkv[...], (((1,), (1,)), ((), ())), preferred_element_type=F32)
     kvt = kv[0:TOK, :].T
     for i in (10, 11, 12, 13):
         loads[i].wait()
@@ -206,29 +222,27 @@
     kg2 = jnp.concatenate([kg[...], kg[...]], axis=1)
     bufa[0, 128:144, :] = jnp.where(lowc, ckv * lax.rsqrt(csq + EPS) * kg2, ckv).astype(BF16)
 
-    def send(src, dst, dev_a, dev_b):
-        remote(bufa.at[src], bufa.at[dst], sa.at[dst], ra.at[dst], dev_a).start()
-        remote(bufb.at[src], bufb.at[dst], sb.at[dst], rb.at[dst], dev_b).start()
-
-    def arrived(s):
-        remote(bufa.at[s], bufa.at[s], sa.at[s], ra.at[s], at_z(1)).wait_recv()
-        remote(bufb.at[s], bufb.at[s], sb.at[s], rb.at[s], at_y(1)).wait_recv()
-
-    def first(dst_, src_, s):
-        send(src_, dst_, at_y(s), at_z(s))
-
-    def second(src_, dst_, s):
-        send(src_, dst_, at_z(s), at_y(s))
-
-    def start_rows(i):
-        nxt = {0: (1, 2), 1: (3,), 2: (4,), 3: (5,), 4: (6,), 5: (7,)}.get(i, ())
-        for t in nxt:
-            first(t, i, sgn if t % 2 == 1 else -sgn)
-        base = (2 + i // 2) * 4 + i % 2
-        second(i, base, sgn)
-        second(i, base + 2, -sgn)
-
-    start_rows(0)
+    def ring(axis, k):
+        along_y = 1 - d if axis == 0 else d
+        k = k * sgn
+        return {
+            "sp": lax.rem(z + (1 - along_y) * k + RING, RING) * RING + lax.rem(y + along_y * k + RING, RING)
+        }
+
+    def group(s):
+        return s if s < 16 else 8 + s // 2
+
+    def pass_on(s):
+        for axis, way, t in onward(ORDER[s]):
+            remote(bufa.at[s], bufa.at[t], sa, ra.at[group(t)], ring(axis, way)).start()
+            remote(bufb.at[s], bufb.at[t], sb, rb.at[group(t)], ring(1 - axis, way)).start()
+
+    def arrived(s, n):
+        pa, pb = bufa.at[s : s + n], bufb.at[s : s + n]
+        remote(pa, pa, sa, ra.at[group(s)], at_z(1)).wait_recv()
+        remote(pb, pb, sb, rb.at[group(s)], at_y(1)).wait_recv()
+
+    pass_on(0)
 
     q = dot(normed[0:TOK, :], wq[...])
     qt = q.T
@@ -245,44 +259,76 @@
         qctx[h, 0:64, :] = hi
         qctx[h, 128:192, :] = lo
 
-    def absorb(h, mnew, rowsum, prod):
-        alpha = jnp.exp2(mst[h] - mnew)
-        mst[h] = mnew
-        lst[h] = lst[h] * alpha[0:1, :] + rowsum
+    sbuf = (sbuf0, sbuf1)
+
+    def keep(keys, h, sref):
+        for t in range(2):
+            sc = dot(keys, qbd[2 * h + t])
+            sref[:, :, t * 256 : (t + 1) * 256] = sc.reshape(4, 128, 256)
+            m = jnp.max(sc.reshape(64, 8, 256), axis=0)
+            m = jnp.maximum(m[:, 0:128], m[:, 128:256])
+            cols = slice(t * 128, (t + 1) * 128)
+            mold = mst[h, :, cols]
+            m = jnp.maximum(jnp.broadcast_to(jnp.max(m, axis=0, keepdims=True), (8, 128)), mold)
+            mst[h, :, cols] = m
+            alp[h, :, cols] = jnp.exp2(mold - m)
+
+    def use(vals, h, sref, zero):
+        m = jnp.concatenate([mst[h, :, 0:128]] * 2 + [mst[h, :, 128:256]] * 2, axis=1)
+        alpha = alp[h]
+        rows = jnp.zeros((8, 512), F32)
+        prod = jnp.zeros((HD, 256), F32)
+        for k in range(4):
+            e = jnp.exp2(sref[k + zero].reshape(16, 8, 512) - m[None])
+            rows = rows + jnp.sum(e, axis=0)
+            pb = e.reshape(128, 512).astype(BF16)
+            p = jnp.concatenate(
+                [
+                    jnp.concatenate([pb[r : r + 64, c : c + 128], pb[r : r + 64, c + 256 : c + 384]], axis=1)
+                    for r in (0, 64)
+                    for c in (0, 128)
+                ],
+                axis=0,
+            )
+            prod = prod + dot(vals[:, 256 * k : 256 * k + 256], p)
+        rows = jnp.concatenate([rows[:, 0:128] + rows[:, 128:256], rows[:, 256:384] + rows[:, 384:512]], axis=1)
+        alp[h] = jnp.ones((8, 256), F32)
+        lst[h] = lst[h] * alpha + rows
         acc[h] = acc[h] * alpha[0:1, :] + prod
+
+    def receive(st):
+        n = 1 if st < 4 else 2
+        for s in range(4 * st, 4 * st + 4, n):
+            if s > 0:
+                arrived(s, n)
+                for t in range(n):
+                    pass_on(s + t)
+
+    def pick(value, low, high):
+        if high - low == 1:
+            receive(low)
+            return
+        mid = (low + high) // 2
+
+        @pl.when(value < mid)
+        def _():
+            pick(value, low, mid)
+
+        @pl.when(value >= mid)
+        def _():
+            pick(value, mid, high)
+
+    def keys_of(base):
+        k = jnp.concatenate(
+            [bufa[pl.ds(base, 4), 0:64, :].reshape(256, 128), bufb[pl.ds(base, 4), 0:64, :].reshape(256, 128)], axis=0
+        )
+        return jnp.concatenate([k, k], axis=1)
 
     def step(it, carry):
         base = it * 4
-
-        @pl.when(it == 0)
-        def _():
-            for i in (1, 2, 3):
-                arrived(i)
-                start_rows(i)
-
-        @pl.when(it == 1)
-        def _():
-            for i in (4, 5, 6, 7):
-                arrived(i)
-                start_rows(i)
-
-        @pl.when((it >= 2) & (it < 10))
-        def _():
-            for k in range(4):
-                arrived(base + k)
-                second(base + k, base + k + 16, sgn if k < 2 else -sgn)
-
-        @pl.when((it >= 10) & (it < 14))
-        def _():
-            for k in range(4):
-                arrived(base + k)
-                if k < 2:
-                    second(base + k, 56 + 2 * (it - 10) + k, sgn)
-
-        @pl.when(it >= 14)
-        def _():
-            for k in range(4):
-                arrived(base + k)
+        zero = jnp.minimum(it, 0)
+
+        pick(it, 0, 16)
 
         @pl.when(it == 8)
         def _():
@@ -302,37 +348,15 @@
             remote(wo.at[far, d, 128:256], wo.at[far, d, 128:256], swo.at[3], rwo.at[3], at_x(-1)).wait()
             remote(wo.at[far, d], wo.at[far, d], swo.at[6], rwo.at[6], partner).start()
 
-        keys = jnp.concatenate(
-            [bufa[pl.ds(base, 4), 0:64, :].reshape(256, 128), bufb[pl.ds(base, 4), 0:64, :].reshape(256, 128)], axis=0
-        )
-        keys = jnp.concatenate([keys, keys], axis=1)
+        keys = keys_of(base)
         vals = jnp.concatenate(
             [bufa[base + k, 64:128, :] for k in range(4)] + [bufb[base + k, 64:128, :] for k in range(4)], axis=1
         )
+        keep(keys, 0, sbuf[0])
         for h in range(NH):
-            ps = []
-            ms = []
-            sums = []
-            mold = mst[h]
-            for t in range(2):
-                s = dot(keys, qbd[2 * h + t])
-                m = jnp.max(s.reshape(64, 8, 256), axis=0)
-                m = jnp.maximum(m[:, 0:128], m[:, 128:256])
-                m = jnp.max(m, axis=0, keepdims=True)
-                m = jnp.maximum(m, mold[0:1, t * 128 : (t + 1) * 128])
-                e = jnp.exp2(s - jnp.concatenate([m, m], axis=1))
-                r = jnp.sum(e.reshape(64, 8, 256), axis=0)
-                sums.append(r[:, 0:128] + r[:, 128:256])
-                ms.append(m)
-                pb = e.astype(BF16)
-                parts = []
-                for k in range(8):
-                    parts.append(pb[64 * k : 64 * k + 64, 0:128])
-                    parts.append(pb[64 * k : 64 * k + 64, 128:256])
-                ps.append(jnp.concatenate(parts, axis=0))
-            prod = dot(vals, jnp.concatenate(ps, axis=1))
-            mnew = jnp.broadcast_to(jnp.concatenate(ms, axis=1), (8, 256))
-            absorb(h, mnew, jnp.concatenate(sums, axis=1), prod)
+            if h + 1 < NH:
+                keep(keys, h + 1, sbuf[(h + 1) % 2])
+            use(vals, h, sbuf[h % 2], zero)
 
         @pl.when(it % 4 == 3)
         def _():
@@ -340,13 +364,20 @@
             cc = jnp.concatenate([c, c], axis=1)
             cvt = c.astype(F32).T[HD:128, :].astype(BF16)
             for h in range(NH):
-                s = dot(cc, qctx[h]) + bias[0:1, h : h + 1] * LOG2E
+                sc = dot(cc, qctx[h]) + bias[0:1, h : h + 1] * LOG2E
+                sctx[h] = sc
+                m = jnp.max(sc.reshape(32, 8, 256), axis=0)
                 mold = mst[h]
-                m = jnp.maximum(jnp.max(s, axis=0, keepdims=True), mold[0:1, :])
-                e = jnp.exp2(s - m)
-                r = jnp.sum(e.reshape(32, 8, 256), axis=0)
-                prod = dot(cvt, e.astype(BF16))
-                absorb(h, jnp.broadcast_to(m, (8, 256)), r, prod)
+                m = jnp.maximum(jnp.broadcast_to(jnp.max(m, axis=0, keepdims=True), (8, 256)), mold)
+                mst[h] = m
+                alp[h] = alp[h] * jnp.exp2(mold - m)
+            for h in range(NH):
+                alpha = alp[h]
+                alp[h] = jnp.ones((8, 256), F32)
+                e = jnp.exp2(sctx[h + zero].reshape(32, 8, 256) - mst[h][None])
+                prod = dot(cvt, e.reshape(256, 256).astype(BF16))
+                lst[h] = lst[h] * alpha + jnp.sum(e, axis=0)
+                acc[h] = acc[h] * alpha[0:1, :] + prod
 
         return carry
 
@@ -369,6 +400,9 @@
     own = [att_copy(x, 0, 0, 1), att_copy(x, 1, 1, -1), att_copy(x, 1, 2, 1), att_copy(x, 0, 3, -1)]
     for c in own:
         c.start()
+    pa, pb = bufa.at[1:64], bufb.at[1:64]
+    remote(pa, pa, sa, ra.at[0], at_z(1)).wait_send()
+    remote(pb, pb, sb, rb.at[0], at_y(1)).wait_send()
     own[0].wait_recv()
     fwd0 = att_copy(left, 0, 4, 1)
     fwd0.start()
@@ -398,12 +432,6 @@
     for c in own:
         c.wait_send()
 
-    def drain(s, carry):
-        remote(bufa.at[s], bufa.at[s], sa.at[s], ra.at[s], at_z(1)).wait_send()
-        remote(bufb.at[s], bufb.at[s], sb.at[s], rb.at[s], at_y(1)).wait_send()
-        return carry
-
-    lax.fori_loop(1, 64, drain, 0)
     for o in outs:
         o.wait()
 
@@ -417,16 +445,17 @@
     scratch = [
         V((TOK, D), BF16), V((1, 32), BF16), V((CTXT, D), BF16), V((1, 32), BF16),
         V((32, 512), BF16), V((32, 512), BF16), V((32, 512), BF16), V((1, D), F32),
-        V((D, QC), BF16), V((D, HD), BF16), V((D, HD), BF16), V((XN, 2, QC, D // 2), BF16),
+        V((D, QC), BF16), V((2 * HD, D), BF16), V((XN, 2, QC, D // 2), BF16),
         V((1, HD), F32), V((1, HD), F32), V((1, NH), F32),
-        V((TOK, D), BF16), V((TOK + CTXT, D), BF16), V((D, 128), BF16),
+        V((TOK, D), BF16), V((TOK + CTXT, D), BF16),
         V((8, 256, 256), BF16), V((NH, 256, 256), BF16),
         V((64, 144, 128), BF16), V((64, 128, 128), BF16),
-        V((NH, 8, 256), F32), V((NH, 8, 256), F32), V((NH, HD, 256), F32), V((XN, TOK, QC), BF16),
+        V((NH, 8, 256), F32), V((NH, 8, 256), F32), V((NH, 8, 256), F32), V((NH, HD, 256), F32), V((XN, TOK, QC), BF16),
+        V((4, 128, 512), F32), V((4, 128, 512), F32), V((NH, 256, 256), F32),
         V((16, 128), F32), V((RING, 16, 128), F32), V((1, 16, 128), F32), V((RING, 16, 128), F32), V((XN, 16, 128), F32),
         V((8, 128), F32), V((RING, 8, 128), F32), V((1, 8, 128), F32), V((RING, 8, 128), F32), V((XN, 8, 128), F32),
-        dma((16,)), dma((8,)), dma((64,)), dma((64,)), dma((64,)), dma((64,)),
-        dma((40,)), dma((40,)), dma((8,)), dma((8,)), dma((8,)), dma((8,)),
+        dma((16,)), dma((8,)), dma, dma((40,)), dma, dma((40,)),
+        dma((6,)), dma((6,)), dma((7,)), dma((7,)), dma((6,)), dma((6,)),
     ]
     out = pl.pallas_call(
         kernel,
@@ -440,7 +469,7 @@
         name="fused",
     )(
         latent[0], condition, context[0], context_code[None], shift_weight, scale_weight, gate_weight,
-        norm_gain[None], query_weight, key_weight, value_weight, output_weight,
+        norm_gain[None], query_weight, key_weight.T, value_weight.T, output_weight,
         query_gain[None], key_gain[None], context_bias[None],
     )
     return out[None]

time: 101 us -> 78.5 us (0.78)
  the two profiles are of different devices: /device:TPU:4 before, /device:TPU:2 now
where the time goes in v2:
time: 78.5 us; the launch traced here: 78.4 us
  Pallas kernels  76.1 us (97%)
  local copies, waits for them, and re-layouts  2.3 us (3%)
    pallas_call x1, Pallas kernels, on_device(): pl.pallas_call(kernel, out_shape=jax.ShapeDtypeStruct((TOK, D), BF16), in...  76.1 us
    unnamed x1, local copies, waits for them, and re-layouts  2.3 us

profile of v2, /device:TPU:2, one launch (start us, length us, event | category | flops | bytes accessed | tf_op | source)
XLA Modules:
  0.0 78.4 jit_solution(17739812002199933689)
XLA Ops:
  0.0 76.1 %fused.1 = bf16[256,2048]{1,0:T(8,128)(2,1)} custom-call(bf16[256,2048]{1,0:T(8,128)(2,1)} %bitcast.11, bf16[1,32]{1,0:T(2,128)(2,1)} %cond_h.1, bf16[16,2048]{1,0:T(8,128)(2,1)} %bitcast.14, bf16[1,32]{1,0:T(2,128)(2,1)} %bitcast.16, bf16[32,512]{1,0:T(8,128)(2,1)} %shw_h.1, bf16[32,512]{1,0:T(8,128)(2,1)} %scw_h.1, bf16[32,512]{1,0:T(8,128)(2,1)} %gaw_h.1, ...), custom_call_target="tpu_custom_call" | custom-call | tf_op jit(solution)/shard_map/fused/pallas_call | solution.py:460
  76.1 2.3 %copy.17 = bf16[1,256,2048]{2,1,0:T(8,128)(2,1)} copy(bf16[1,256,2048]{2,1,0:T(8,128)(2,1)} %bitcast.10) | data formatting | bytes 2097152

commit v3 on v2

--- a/solution.py
+++ b/solution.py
@@ -26,11 +26,11 @@
 
 
 ORDER = [
-    (0, 0), (1, 0), (2, 0), (0, -1), (0, 1), (4, 0), (3, 0), (1, 1), (1, -1), (2, -1), (2, 1), (0, 2), (0, -2),
-    (5, 0), (6, 0), (3, -1), (3, 1), (4, -1), (4, 1), (1, 2), (1, -2), (5, -1), (7, 0), (5, 1), (6, -1), (2, -2),
-    (6, 1), (3, -2), (2, 2), (7, -1), (7, 1), (4, -2), (3, 2), (5, -2), (4, 2), (6, -2), (5, 2), (7, -2), (6, 2),
-    (0, -3), (7, 2), (1, -3), (0, 3), (1, 3), (2, -3), (3, -3), (2, 3), (4, -3), (3, 3), (4, 3), (5, -3), (5, 3),
-    (6, -3), (7, -3), (6, 3), (7, 3), (0, 4), (1, 4), (2, 4), (3, 4), (4, 4), (5, 4), (6, 4), (7, 4),
+    (0, 0), (2, 0), (1, 0), (0, -1), (0, 1), (4, 0), (2, -1), (3, 0), (2, 1), (1, 1), (1, -1), (0, -2), (5, 0),
+    (6, 0), (4, -1), (4, 1), (3, -1), (2, -2), (3, 1), (0, 2), (7, 0), (1, 2), (1, -2), (0, -3), (6, 1), (5, 1),
+    (6, -1), (2, 2), (4, -2), (5, -1), (3, -2), (4, 2), (1, -3), (2, -3), (7, 1), (7, -1), (6, 2), (0, 3),
+    (6, -2), (3, 2), (5, 2), (4, -3), (1, 3), (2, 3), (7, -2), (7, 2), (5, -2), (4, 3), (3, 3), (6, -3), (6, 3),
+    (5, 3), (7, 3), (7, -3), (0, 4), (1, 4), (4, 4), (2, 4), (3, -3), (3, 4), (6, 4), (5, 4), (7, 4), (5, -3),
 ]
 SLOT = {item: n for n, item in enumerate(ORDER)}
 NEXT = {0: ((1, 1), (2, -1)), 1: ((3, 1),), 2: ((4, -1),), 3: ((5, 1),), 4: ((6, -1),), 5: ((7, 1),)}
@@ -56,8 +56,8 @@
     latent_h, cond_h, context_h, code_h, shw_h, scw_h, gaw_h, ngain_h, wq_h, wk_h, wv_h, wo_h, qg_h, kg_h, bias_h,
     out_h,
     lat, cond, ctx, code, shw, scw, gaw, ngain, wq, wkv, wo, qg, kg, bias,
-    outv, normed, qbd, qctx, bufa, bufb, mst, alp, lst, acc, att, sbuf0, sbuf1, sctx,
-    ma, ma_y, ma_s, ma_z, ma_x, mb, mb_z, mb_s, mb_y, mb_x,
+    outv, normed, qbd, qctx, bufa, bufb, mst, alp, acc, att, sbuf0, sbuf1, sctx,
+    ma, ma_y, ma_s, ma_z, ma_x, mg, mg_y, mg_s, mg_z, mg_x, mb, mb_z, mb_s, mb_y, mb_x,
     lsem, osem, sa, ra, sb, rb, smod, rmod, swo, rwo, satt, ratt,
 ):
     sp = lax.axis_index("sp")
@@ -112,10 +112,10 @@
         cols = slice(c * 128, (c + 1) * 128)
         ma[c : c + 1, :] = pshift[0:1, cols]
         ma[4 + c : 5 + c, :] = pscale[0:1, cols]
-        ma[8 + c : 9 + c, :] = pgate[0:1, cols]
+        mg[c : c + 1, :] = pgate[0:1, cols]
         mb[c : c + 1, :] = pshift[1:2, cols]
         mb[4 + c : 5 + c, :] = pscale[1:2, cols]
-    ma[12:16, :] = jnp.zeros((4, 128), F32)
+    mg[4:8, :] = jnp.zeros((4, 128), F32)
 
     pl.semaphore_wait(barrier, 2 * (RING - 1) + (XN - 1) + 1)
 
@@ -129,15 +129,6 @@
 
     spread(ma, ma_y, 0, at_y)
     spread(mb, mb_z, 1, at_z)
-
-    for i in (14, 15):
-        loads[i].wait()
-    wo1 = [
-        remote(wo.at[x, d], wo.at[x, d], swo.at[0], rwo.at[0], at_x(1)),
-        remote(wo.at[x, d], wo.at[x, d], swo.at[1], rwo.at[1], at_x(-1)),
-    ]
-    for c in wo1:
-        c.start()
 
     for i in (5, 6, 7, 8, 9):
         loads[i].wait()
@@ -148,7 +139,6 @@
     qbd[...] = jnp.zeros(qbd.shape, BF16)
     qctx[...] = jnp.zeros(qctx.shape, BF16)
     mst[...] = jnp.full(mst.shape, -1e30, F32)
-    lst[...] = jnp.zeros(lst.shape, F32)
     acc[...] = jnp.zeros(acc.shape, F32)
     fi = lax.broadcasted_iota(jnp.int32, (32, TOK), 0)
     ti = lax.broadcasted_iota(jnp.int32, (32, TOK), 1)
@@ -243,6 +233,16 @@
         remote(pb, pb, sb, rb.at[group(s)], at_y(1)).wait_recv()
 
     pass_on(0)
+    spread(mg, mg_y, 6, at_y)
+    for i in (14, 15):
+        loads[i].wait()
+    wo1 = [
+        remote(wo.at[x, d], wo.at[x, d], swo.at[0], rwo.at[0], at_x(1)),
+        remote(wo.at[x, d], wo.at[x, d], swo.at[1], rwo.at[1], at_x(-1)),
+    ]
+    for c in wo1:
+        c.start()
+
 
     q = dot(normed[0:TOK, :], wq[...])
     qt = q.T
@@ -276,11 +276,9 @@
     def use(vals, h, sref, zero):
         m = jnp.concatenate([mst[h, :, 0:128]] * 2 + [mst[h, :, 128:256]] * 2, axis=1)
         alpha = alp[h]
-        rows = jnp.zeros((8, 512), F32)
-        prod = jnp.zeros((HD, 256), F32)
+        prod = jnp.zeros((HD + 16, 256), F32)
         for k in range(4):
             e = jnp.exp2(sref[k + zero].reshape(16, 8, 512) - m[None])
-            rows = rows + jnp.sum(e, axis=0)
             pb = e.reshape(128, 512).astype(BF16)
             p = jnp.concatenate(
                 [
@@ -291,9 +289,7 @@
                 axis=0,
             )
             prod = prod + dot(vals[:, 256 * k : 256 * k + 256], p)
-        rows = jnp.concatenate([rows[:, 0:128] + rows[:, 128:256], rows[:, 256:384] + rows[:, 384:512]], axis=1)
         alp[h] = jnp.ones((8, 256), F32)
-        lst[h] = lst[h] * alpha + rows
         acc[h] = acc[h] * alpha[0:1, :] + prod
 
     def receive(st):
@@ -329,6 +325,25 @@
         zero = jnp.minimum(it, 0)
 
         pick(it, 0, 16)
+
+        @pl.when(it == 5)
+        def _():
+            spread_wait(mg_y, 6)
+            tg = mg[...]
+            for k in range(1, RING):
+                tg = tg + mg_y[k]
+            mg_s[0] = tg
+            spread(mg_s.at[0], mg_z, 7, at_z)
+
+        @pl.when(it == 12)
+        def _():
+            spread_wait(mg_z, 7)
+            tg = mg_s[0]
+            for k in range(1, RING):
+                tg = tg + mg_z[k]
+            mg_x[x] = tg
+            for k in range(1, XN):
+                remote(mg_x.at[x], mg_x.at[x], smod.at[8], rmod.at[8], at_x(k)).start()
 
         @pl.when(it == 8)
         def _():
@@ -352,6 +367,7 @@
         vals = jnp.concatenate(
             [bufa[base + k, 64:128, :] for k in range(4)] + [bufb[base + k, 64:128, :] for k in range(4)], axis=1
         )
+        vals = jnp.concatenate([vals, jnp.ones((16, 1024), BF16)], axis=0)
         keep(keys, 0, sbuf[0])
         for h in range(NH):
             if h + 1 < NH:
@@ -362,7 +378,7 @@
         def _():
             c = bufa[pl.ds(base - 12, 16), 128:144, :].reshape(256, 128)
             cc = jnp.concatenate([c, c], axis=1)
-            cvt = c.astype(F32).T[HD:128, :].astype(BF16)
+            cvt = jnp.concatenate([c.astype(F32).T[HD:128, :].astype(BF16), jnp.ones((16, 256), BF16)], axis=0)
             for h in range(NH):
                 sc = dot(cc, qctx[h]) + bias[0:1, h : h + 1] * LOG2E
                 sctx[h] = sc
@@ -376,7 +392,6 @@
                 alp[h] = jnp.ones((8, 256), F32)
                 e = jnp.exp2(sctx[h + zero].reshape(32, 8, 256) - mst[h][None])
                 prod = dot(cvt, e.reshape(256, 256).astype(BF16))
-                lst[h] = lst[h] * alpha + jnp.sum(e, axis=0)
                 acc[h] = acc[h] * alpha[0:1, :] + prod
 
         return carry
@@ -385,8 +400,7 @@
 
     heads = []
     for h in range(NH):
-        total = jnp.sum(lst[h], axis=0, keepdims=True)
-        heads.append(acc[h] / total)
+        heads.append(acc[h, 0:HD] / acc[h, HD : HD + 1])
     att[x] = jnp.concatenate(heads, axis=0).T.astype(BF16)
 
     left = lax.rem(x + XN - 1, XN)
@@ -416,7 +430,9 @@
     fwd0.wait()
     fwd1.wait()
 
-    gate = vec(ma_x, 8)
+    piece = mg_x.at[1:XN]
+    remote(piece, piece, smod.at[8], rmod.at[8], at_x(1)).wait()
+    gate = vec(mg_x, 0)
     outs = []
     for c in range(8):
         side, off = c // 4, (c % 4) * 256
@@ -450,12 +466,13 @@
         V((TOK, D), BF16), V((TOK + CTXT, D), BF16),
         V((8, 256, 256), BF16), V((NH, 256, 256), BF16),
         V((64, 144, 128), BF16), V((64, 128, 128), BF16),
-        V((NH, 8, 256), F32), V((NH, 8, 256), F32), V((NH, 8, 256), F32), V((NH, HD, 256), F32), V((XN, TOK, QC), BF16),
+        V((NH, 8, 256), F32), V((NH, 8, 256), F32), V((NH, HD + 16, 256), F32), V((XN, TOK, QC), BF16),
         V((4, 128, 512), F32), V((4, 128, 512), F32), V((NH, 256, 256), F32),
-        V((16, 128), F32), V((RING, 16, 128), F32), V((1, 16, 128), F32), V((RING, 16, 128), F32), V((XN, 16, 128), F32),
+        V((8, 128), F32), V((RING, 8, 128), F32), V((1, 8, 128), F32), V((RING, 8, 128), F32), V((XN, 8, 128), F32),
+        V((8, 128), F32), V((RING, 8, 128), F32), V((1, 8, 128), F32), V((RING, 8, 128), F32), V((XN, 8, 128), F32),
         V((8, 128), F32), V((RING, 8, 128), F32), V((1, 8, 128), F32), V((RING, 8, 128), F32), V((XN, 8, 128), F32),
         dma((16,)), dma((8,)), dma, dma((40,)), dma, dma((40,)),
-        dma((6,)), dma((6,)), dma((7,)), dma((7,)), dma((6,)), dma((6,)),
+        dma((9,)), dma((9,)), dma((7,)), dma((7,)), dma((6,)), dma((6,)),
     ]
     out = pl.pallas_call(
         kernel,

time: 78.5 us -> 74.6 us (0.950)
  Pallas kernels: 76.1 us -> 72.1 us
    pallas_call x1, Pallas kernels: 76.1 us -> 72.1 us  [on_device(): pl.pallas_call(kernel, out_shape=jax.ShapeDtypeStruct((TOK, D), BF16), in...]
where the time goes in v3:
time: 74.6 us; the launch traced here: 74.4 us
  Pallas kernels  72.1 us (97%)
  local copies, waits for them, and re-layouts  2.3 us (3%)
    pallas_call x1, Pallas kernels, on_device(): pl.pallas_call(kernel, out_shape=jax.ShapeDtypeStruct((TOK, D), BF16), in...  72.1 us
    unnamed x1, local copies, waits for them, and re-layouts  2.3 us

profile of v3, /device:TPU:2, one launch (start us, length us, event | category | flops | bytes accessed | tf_op | source)
XLA Modules:
  0.0 74.4 jit_solution(17263958208092276096)
XLA Ops:
  0.0 72.1 %fused.1 = bf16[256,2048]{1,0:T(8,128)(2,1)} custom-call(bf16[256,2048]{1,0:T(8,128)(2,1)} %bitcast.11, bf16[1,32]{1,0:T(2,128)(2,1)} %cond_h.1, bf16[16,2048]{1,0:T(8,128)(2,1)} %bitcast.14, bf16[1,32]{1,0:T(2,128)(2,1)} %bitcast.16, bf16[32,512]{1,0:T(8,128)(2,1)} %shw_h.1, bf16[32,512]{1,0:T(8,128)(2,1)} %scw_h.1, bf16[32,512]{1,0:T(8,128)(2,1)} %gaw_h.1, ...), custom_call_target="tpu_custom_call" | custom-call | tf_op jit(solution)/shard_map/fused/pallas_call | solution.py:477
  72.1 2.3 %copy.17 = bf16[1,256,2048]{2,1,0:T(8,128)(2,1)} copy(bf16[1,256,2048]{2,1,0:T(8,128)(2,1)} %bitcast.10) | data formatting | bytes 2097152

commit v4 on v3

--- a/solution.py
+++ b/solution.py
@@ -56,9 +56,9 @@
     latent_h, cond_h, context_h, code_h, shw_h, scw_h, gaw_h, ngain_h, wq_h, wk_h, wv_h, wo_h, qg_h, kg_h, bias_h,
     out_h,
     lat, cond, ctx, code, shw, scw, gaw, ngain, wq, wkv, wo, qg, kg, bias,
-    outv, normed, qbd, qctx, bufa, bufb, mst, alp, acc, att, sbuf0, sbuf1, sctx,
+    outv, normed, qbd, qctx, buf, mst, alp, acc, att, sbuf0, sbuf1, cbuf0, cbuf1,
     ma, ma_y, ma_s, ma_z, ma_x, mg, mg_y, mg_s, mg_z, mg_x, mb, mb_z, mb_s, mb_y, mb_x,
-    lsem, osem, sa, ra, sb, rb, smod, rmod, swo, rwo, satt, ratt,
+    lsem, osem, sa, ra, smod, rmod, swo, rwo, satt, ratt,
 ):
     sp = lax.axis_index("sp")
     x = lax.axis_index("tp")
@@ -82,6 +82,14 @@
         return pltpu.make_async_remote_copy(
             src_ref=src, dst_ref=dst, send_sem=ss, recv_sem=rs, device_id=dev, device_id_type=MESH
         )
+
+    barrier = pltpu.get_barrier_semaphore()
+    for k in range(1, RING):
+        pl.semaphore_signal(barrier, inc=1, device_id=at_y(k), device_id_type=MESH)
+        pl.semaphore_signal(barrier, inc=1, device_id=at_z(k), device_id_type=MESH)
+    for k in range(1, XN):
+        pl.semaphore_signal(barrier, inc=1, device_id=at_x(k), device_id_type=MESH)
+    pl.semaphore_signal(barrier, inc=1, device_id=partner, device_id_type=MESH)
 
     pairs = [
         (cond_h, cond), (code_h, code), (shw_h, shw), (scw_h, scw), (gaw_h, gaw),
@@ -92,14 +100,6 @@
     loads = [pltpu.make_async_copy(s, t, lsem.at[i]) for i, (s, t) in enumerate(pairs)]
     for c in loads:
         c.start()
-
-    barrier = pltpu.get_barrier_semaphore()
-    for k in range(1, RING):
-        pl.semaphore_signal(barrier, inc=1, device_id=at_y(k), device_id_type=MESH)
-        pl.semaphore_signal(barrier, inc=1, device_id=at_z(k), device_id_type=MESH)
-    for k in range(1, XN):
-        pl.semaphore_signal(barrier, inc=1, device_id=at_x(k), device_id_type=MESH)
-    pl.semaphore_signal(barrier, inc=1, device_id=partner, device_id_type=MESH)
 
     for i in range(5):
         loads[i].wait()
@@ -202,15 +202,15 @@
     k2 = jnp.concatenate([kt, kt], axis=0).T
     low = lax.broadcasted_iota(jnp.int32, (HD, 128), 1) < HD
     vt = kvt[HD : 2 * HD, :].astype(BF16)
-    bufa[0, 0:64, :] = jnp.where(low, k2[0:64], k2[64:128]).astype(BF16)
-    bufb[0, 0:64, :] = jnp.where(low, k2[128:192], k2[192:256]).astype(BF16)
-    bufa[0, 64:128, :] = vt[:, 0:128]
-    bufb[0, 64:128, :] = vt[:, 128:256]
+    buf[0, 0:64, :] = jnp.where(low, k2[0:64], k2[64:128]).astype(BF16)
+    buf[0, 144:208, :] = jnp.where(low, k2[128:192], k2[192:256]).astype(BF16)
+    buf[0, 64:128, :] = vt[:, 0:128]
+    buf[0, 208:272, :] = vt[:, 128:256]
     ckv = kv[TOK : TOK + CTXT, :]
     lowc = lax.broadcasted_iota(jnp.int32, (CTXT, 128), 1) < HD
     csq = jnp.sum(jnp.where(lowc, ckv * ckv, 0.0), axis=1, keepdims=True) * (1.0 / HD)
     kg2 = jnp.concatenate([kg[...], kg[...]], axis=1)
-    bufa[0, 128:144, :] = jnp.where(lowc, ckv * lax.rsqrt(csq + EPS) * kg2, ckv).astype(BF16)
+    buf[0, 128:144, :] = jnp.where(lowc, ckv * lax.rsqrt(csq + EPS) * kg2, ckv).astype(BF16)
 
     def ring(axis, k):
         along_y = 1 - d if axis == 0 else d
@@ -224,13 +224,12 @@
 
     def pass_on(s):
         for axis, way, t in onward(ORDER[s]):
-            remote(bufa.at[s], bufa.at[t], sa, ra.at[group(t)], ring(axis, way)).start()
-            remote(bufb.at[s], bufb.at[t], sb, rb.at[group(t)], ring(1 - axis, way)).start()
+            remote(buf.at[s, 0:144], buf.at[t, 0:144], sa, ra.at[group(t)], ring(axis, way)).start()
+            remote(buf.at[s, 144:272], buf.at[t, 144:272], sa, ra.at[group(t)], ring(1 - axis, way)).start()
 
     def arrived(s, n):
-        pa, pb = bufa.at[s : s + n], bufb.at[s : s + n]
-        remote(pa, pa, sa, ra.at[group(s)], at_z(1)).wait_recv()
-        remote(pb, pb, sb, rb.at[group(s)], at_y(1)).wait_recv()
+        part = buf.at[s : s + n]
+        remote(part, part, sa, ra.at[group(s)], at_z(1)).wait_recv()
 
     pass_on(0)
     spread(mg, mg_y, 6, at_y)
@@ -260,25 +259,30 @@
         qctx[h, 128:192, :] = lo
 
     sbuf = (sbuf0, sbuf1)
-
-    def keep(keys, h, sref):
+    cbuf = (cbuf0, cbuf1)
+
+    def keep(keys, ctxs, h, n):
+        sc = dot(ctxs, qctx[h]) + bias[0:1, h : h + 1] * LOG2E
+        cbuf[n][0] = sc
+        mc = jnp.max(sc.reshape(8, 8, 256), axis=0)
         for t in range(2):
             sc = dot(keys, qbd[2 * h + t])
-            sref[:, :, t * 256 : (t + 1) * 256] = sc.reshape(4, 128, 256)
+            sbuf[n][:, :, t * 256 : (t + 1) * 256] = sc.reshape(4, 128, 256)
             m = jnp.max(sc.reshape(64, 8, 256), axis=0)
-            m = jnp.maximum(m[:, 0:128], m[:, 128:256])
             cols = slice(t * 128, (t + 1) * 128)
+            m = jnp.maximum(jnp.maximum(m[:, 0:128], m[:, 128:256]), mc[:, cols])
             mold = mst[h, :, cols]
             m = jnp.maximum(jnp.broadcast_to(jnp.max(m, axis=0, keepdims=True), (8, 128)), mold)
             mst[h, :, cols] = m
             alp[h, :, cols] = jnp.exp2(mold - m)
 
-    def use(vals, h, sref, zero):
-        m = jnp.concatenate([mst[h, :, 0:128]] * 2 + [mst[h, :, 128:256]] * 2, axis=1)
-        alpha = alp[h]
-        prod = jnp.zeros((HD + 16, 256), F32)
+    def use(vals, cvals, h, n, zero):
+        m = mst[h]
+        e = jnp.exp2(cbuf[n][zero].reshape(8, 8, 256) - m[None])
+        prod = dot(cvals, e.reshape(64, 256).astype(BF16))
+        m = jnp.concatenate([m[:, 0:128]] * 2 + [m[:, 128:256]] * 2, axis=1)
         for k in range(4):
-            e = jnp.exp2(sref[k + zero].reshape(16, 8, 512) - m[None])
+            e = jnp.exp2(sbuf[n][k + zero].reshape(16, 8, 512) - m[None])
             pb = e.reshape(128, 512).astype(BF16)
             p = jnp.concatenate(
                 [
@@ -289,8 +293,7 @@
                 axis=0,
             )
             prod = prod + dot(vals[:, 256 * k : 256 * k + 256], p)
-        alp[h] = jnp.ones((8, 256), F32)
-        acc[h] = acc[h] * alpha[0:1, :] + prod
+        acc[h] = acc[h] * alp[h, 0:1, :] + prod
 
     def receive(st):
         n = 1 if st < 4 else 2
@@ -316,7 +319,7 @@
 
     def keys_of(base):
         k = jnp.concatenate(
-            [bufa[pl.ds(base, 4), 0:64, :].reshape(256, 128), bufb[pl.ds(base, 4), 0:64, :].reshape(256, 128)], axis=0
+            [buf[pl.ds(base, 4), 0:64, :].reshape(256, 128), buf[pl.ds(base, 4), 144:208, :].reshape(256, 128)], axis=0
         )
         return jnp.concatenate([k, k], axis=1)
 
@@ -365,34 +368,17 @@
 
         keys = keys_of(base)
         vals = jnp.concatenate(
-            [bufa[base + k, 64:128, :] for k in range(4)] + [bufb[base + k, 64:128, :] for k in range(4)], axis=1
+            [buf[base + k, 64:128, :] for k in range(4)] + [buf[base + k, 208:272, :] for k in range(4)], axis=1
         )
         vals = jnp.concatenate([vals, jnp.ones((16, 1024), BF16)], axis=0)
-        keep(keys, 0, sbuf[0])
+        ctxs = buf[pl.ds(base, 4), 128:144, :].reshape(64, 128)
+        cvals = jnp.concatenate([ctxs.astype(F32).T[HD:128, :].astype(BF16), jnp.ones((16, 64), BF16)], axis=0)
+        ctxs = jnp.concatenate([ctxs, ctxs], axis=1)
+        keep(keys, ctxs, 0, 0)
         for h in range(NH):
             if h + 1 < NH:
-                keep(keys, h + 1, sbuf[(h + 1) % 2])
-            use(vals, h, sbuf[h % 2], zero)
-
-        @pl.when(it % 4 == 3)
-        def _():
-            c = bufa[pl.ds(base - 12, 16), 128:144, :].reshape(256, 128)
-            cc = jnp.concatenate([c, c], axis=1)
-            cvt = jnp.concatenate([c.astype(F32).T[HD:128, :].astype(BF16), jnp.ones((16, 256), BF16)], axis=0)
-            for h in range(NH):
-                sc = dot(cc, qctx[h]) + bias[0:1, h : h + 1] * LOG2E
-                sctx[h] = sc
-                m = jnp.max(sc.reshape(32, 8, 256), axis=0)
-                mold = mst[h]
-                m = jnp.maximum(jnp.broadcast_to(jnp.max(m, axis=0, keepdims=True), (8, 256)), mold)
-                mst[h] = m
-                alp[h] = alp[h] * jnp.exp2(mold - m)
-            for h in range(NH):
-                alpha = alp[h]
-                alp[h] = jnp.ones((8, 256), F32)
-                e = jnp.exp2(sctx[h + zero].reshape(32, 8, 256) - mst[h][None])
-                prod = dot(cvt, e.reshape(256, 256).astype(BF16))
-                acc[h] = acc[h] * alpha[0:1, :] + prod
+                keep(keys, ctxs, h + 1, (h + 1) % 2)
+            use(vals, cvals, h, h % 2, zero)
 
         return carry
 
@@ -414,9 +400,8 @@
     own = [att_copy(x, 0, 0, 1), att_copy(x, 1, 1, -1), att_copy(x, 1, 2, 1), att_copy(x, 0, 3, -1)]
     for c in own:
         c.start()
-    pa, pb = bufa.at[1:64], bufb.at[1:64]
-    remote(pa, pa, sa, ra.at[0], at_z(1)).wait_send()
-    remote(pb, pb, sb, rb.at[0], at_y(1)).wait_send()
+    part = buf.at[1:64]
+    remote(part, part, sa, ra.at[0], at_z(1)).wait_send()
     own[0].wait_recv()
     fwd0 = att_copy(left, 0, 4, 1)
     fwd0.start()
@@ -433,7 +418,6 @@
     piece = mg_x.at[1:XN]
     remote(piece, piece, smod.at[8], rmod.at[8], at_x(1)).wait()
     gate = vec(mg_x, 0)
-    outs = []
     for c in range(8):
         side, off = c // 4, (c % 4) * 256
         mixed = jnp.zeros((TOK, 256), F32)
@@ -441,15 +425,12 @@
             mixed = mixed + dot(att[g], wo[g, side, :, off : off + 256]).astype(BF16).astype(F32)
         cols = slice(c * 256, (c + 1) * 256)
         outv[:, cols] = (lat[:, cols].astype(F32) + gate[:, cols] * mixed).astype(BF16)
-        o = pltpu.make_async_copy(outv.at[:, cols], out_h.at[:, cols], osem.at[c])
-        o.start()
-        outs.append(o)
+        pltpu.make_async_copy(outv.at[:, cols], out_h.at[:, cols], osem).start()
 
     for c in own:
         c.wait_send()
 
-    for o in outs:
-        o.wait()
+    pltpu.make_async_copy(outv, out_h, osem).wait()
 
 
 def on_device(
@@ -465,13 +446,13 @@
         V((1, HD), F32), V((1, HD), F32), V((1, NH), F32),
         V((TOK, D), BF16), V((TOK + CTXT, D), BF16),
         V((8, 256, 256), BF16), V((NH, 256, 256), BF16),
-        V((64, 144, 128), BF16), V((64, 128, 128), BF16),
+        V((64, 272, 128), BF16),
         V((NH, 8, 256), F32), V((NH, 8, 256), F32), V((NH, HD + 16, 256), F32), V((XN, TOK, QC), BF16),
-        V((4, 128, 512), F32), V((4, 128, 512), F32), V((NH, 256, 256), F32),
+        V((4, 128, 512), F32), V((4, 128, 512), F32), V((1, 64, 256), F32), V((1, 64, 256), F32),
         V((8, 128), F32), V((RING, 8, 128), F32), V((1, 8, 128), F32), V((RING, 8, 128), F32), V((XN, 8, 128), F32),
         V((8, 128), F32), V((RING, 8, 128), F32), V((1, 8, 128), F32), V((RING, 8, 128), F32), V((XN, 8, 128), F32),
         V((8, 128), F32), V((RING, 8, 128), F32), V((1, 8, 128), F32), V((RING, 8, 128), F32), V((XN, 8, 128), F32),
-        dma((16,)), dma((8,)), dma, dma((40,)), dma, dma((40,)),
+        dma((16,)), dma, dma, dma((40,)),
         dma((9,)), dma((9,)), dma((7,)), dma((7,)), dma((6,)), dma((6,)),
     ]
     out = pl.pallas_call(

time: 74.6 us -> 73.4 us (0.984)
  Pallas kernels: 72.1 us -> 71 us
    pallas_call x1, Pallas kernels: 72.1 us -> 71 us  [on_device(): pl.pallas_call(kernel, out_shape=jax.ShapeDtypeStruct((TOK, D), BF16), in...]
where the time goes in v4:
time: 73.4 us; the launch traced here: 73.3 us
  Pallas kernels  71 us (97%)
  local copies, waits for them, and re-layouts  2.3 us (3%)
    pallas_call x1, Pallas kernels, on_device(): pl.pallas_call(kernel, out_shape=jax.ShapeDtypeStruct((TOK, D), BF16), in...  71 us
    unnamed x1, local copies, waits for them, and re-layouts  2.3 us

profile of v4, /device:TPU:2, one launch (start us, length us, event | category | flops | bytes accessed | tf_op | source)
XLA Modules:
  0.0 73.3 jit_solution(13938720695710767241)
XLA Ops:
  0.0 71.0 %fused.1 = bf16[256,2048]{1,0:T(8,128)(2,1)} custom-call(bf16[256,2048]{1,0:T(8,128)(2,1)} %bitcast.11, bf16[1,32]{1,0:T(2,128)(2,1)} %cond_h.1, bf16[16,2048]{1,0:T(8,128)(2,1)} %bitcast.14, bf16[1,32]{1,0:T(2,128)(2,1)} %bitcast.16, bf16[32,512]{1,0:T(8,128)(2,1)} %shw_h.1, bf16[32,512]{1,0:T(8,128)(2,1)} %scw_h.1, bf16[32,512]{1,0:T(8,128)(2,1)} %gaw_h.1, ...), custom_call_target="tpu_custom_call" | custom-call | tf_op jit(solution)/shard_map/fused/pallas_call | solution.py:458
  71.0 2.3 %copy.17 = bf16[1,256,2048]{2,1,0:T(8,128)(2,1)} copy(bf16[1,256,2048]{2,1,0:T(8,128)(2,1)} %bitcast.10) | data formatting | bytes 2097152

commit v5 on v4

--- a/solution.py
+++ b/solution.py
@@ -56,7 +56,7 @@
     latent_h, cond_h, context_h, code_h, shw_h, scw_h, gaw_h, ngain_h, wq_h, wk_h, wv_h, wo_h, qg_h, kg_h, bias_h,
     out_h,
     lat, cond, ctx, code, shw, scw, gaw, ngain, wq, wkv, wo, qg, kg, bias,
-    outv, normed, qbd, qctx, buf, mst, alp, acc, att, sbuf0, sbuf1, cbuf0, cbuf1,
+    outv, normed, qbd, qctx, buf, mst, alp, acc, att, sbuf0, sbuf1, sbuf2, cbuf0, cbuf1, cbuf2,
     ma, ma_y, ma_s, ma_z, ma_x, mg, mg_y, mg_s, mg_z, mg_x, mb, mb_z, mb_s, mb_y, mb_x,
     lsem, osem, sa, ra, smod, rmod, swo, rwo, satt, ratt,
 ):
@@ -258,8 +258,8 @@
         qctx[h, 0:64, :] = hi
         qctx[h, 128:192, :] = lo
 
-    sbuf = (sbuf0, sbuf1)
-    cbuf = (cbuf0, cbuf1)
+    sbuf = (sbuf0, sbuf1, sbuf2)
+    cbuf = (cbuf0, cbuf1, cbuf2)
 
     def keep(keys, ctxs, h, n):
         sc = dot(ctxs, qctx[h]) + bias[0:1, h : h + 1] * LOG2E
@@ -375,10 +375,11 @@
         cvals = jnp.concatenate([ctxs.astype(F32).T[HD:128, :].astype(BF16), jnp.ones((16, 64), BF16)], axis=0)
         ctxs = jnp.concatenate([ctxs, ctxs], axis=1)
         keep(keys, ctxs, 0, 0)
+        keep(keys, ctxs, 1, 1)
         for h in range(NH):
-            if h + 1 < NH:
-                keep(keys, ctxs, h + 1, (h + 1) % 2)
-            use(vals, cvals, h, h % 2, zero)
+            if h + 2 < NH:
+                keep(keys, ctxs, h + 2, (h + 2) % 3)
+            use(vals, cvals, h, h % 3, zero)
 
         return carry
 
@@ -448,7 +449,7 @@
         V((8, 256, 256), BF16), V((NH, 256, 256), BF16),
         V((64, 272, 128), BF16),
         V((NH, 8, 256), F32), V((NH, 8, 256), F32), V((NH, HD + 16, 256), F32), V((XN, TOK, QC), BF16),
-        V((4, 128, 512), F32), V((4, 128, 512), F32), V((1, 64, 256), F32), V((1, 64, 256), F32),
+        V((4, 128, 512), F32), V((4, 128, 512), F32), V((4, 128, 512), F32), V((1, 64, 256), F32), V((1, 64, 256), F32), V((1, 64, 256), F32),
         V((8, 128), F32), V((RING, 8, 128), F32), V((1, 8, 128), F32), V((RING, 8, 128), F32), V((XN, 8, 128), F32),
         V((8, 128), F32), V((RING, 8, 128), F32), V((1, 8, 128), F32), V((RING, 8, 128), F32), V((XN, 8, 128), F32),
         V((8, 128), F32), V((RING, 8, 128), F32), V((1, 8, 128), F32), V((RING, 8, 128), F32), V((XN, 8, 128), F32),

time: 73.4 us -> 73.3 us (level)
  no operation moved by 1% of the time
where the time goes in v5:
time: 73.3 us; the launch traced here: 73.1 us
  Pallas kernels  70.8 us (97%)
  local copies, waits for them, and re-layouts  2.3 us (3%)
    pallas_call x1, Pallas kernels, on_device(): pl.pallas_call(kernel, out_shape=jax.ShapeDtypeStruct((TOK, D), BF16), in...  70.8 us
    unnamed x1, local copies, waits for them, and re-layouts  2.3 us

profile of v5, /device:TPU:2, one launch (start us, length us, event | category | flops | bytes accessed | tf_op | source)
XLA Modules:
  0.0 73.1 jit_solution(8992770136698378718)
XLA Ops:
  0.0 70.8 %fused.1 = bf16[256,2048]{1,0:T(8,128)(2,1)} custom-call(bf16[256,2048]{1,0:T(8,128)(2,1)} %bitcast.11, bf16[1,32]{1,0:T(2,128)(2,1)} %cond_h.1, bf16[16,2048]{1,0:T(8,128)(2,1)} %bitcast.14, bf16[1,32]{1,0:T(2,128)(2,1)} %bitcast.16, bf16[32,512]{1,0:T(8,128)(2,1)} %shw_h.1, bf16[32,512]{1,0:T(8,128)(2,1)} %scw_h.1, bf16[32,512]{1,0:T(8,128)(2,1)} %gaw_h.1, ...), custom_call_target="tpu_custom_call" | custom-call | tf_op jit(solution)/shard_map/fused/pallas_call | solution.py:459
  70.8 2.3 %copy.17 = bf16[1,256,2048]{2,1,0:T(8,128)(2,1)} copy(bf16[1,256,2048]{2,1,0:T(8,128)(2,1)} %bitcast.10) | data formatting | bytes 2097152
